TPU v7x, 256 devices: a whole 4x4x8 slice. The times are simulated.
256 devices in a mesh: fs: 32 (over z, y), tp: 8 (over x, core).
Axes of the slice: x: 4, y: 4, z: 8, core: 2. Of those that a mesh axis runs over, the one named last changes fastest.
Arguments:
- latent_in: bfloat16 [98304, 512], P('fs'), may hold values from -6 to 6
- query_cot: bfloat16 [98304, 1536], P('fs', 'tp'), may hold values from -6 to 6
- attn_out: bfloat16 [98304, 1024], P('fs'), may hold values from -6 to 6
- mix_cot: bfloat16 [98304, 2048], P('fs', 'tp'), may hold values from -6 to 6
- query_weight: float32 [512, 1536], P('fs', 'tp'), may hold values from -0.25 to 0.25
- output_weight: float32 [1024, 2048], P('fs', 'tp'), may hold values from -0.1875 to 0.1875
- query_factor: bfloat16 [512, 256], P('fs'), may hold values from -0.25 to 0.25
- output_factor: bfloat16 [1024, 256], P('fs'), may hold values from -0.1875 to 0.1875
- query_mean: float32 [256, 1536], P('fs', 'tp'), may hold values from -3 to 3
- query_square: float32 [256, 1536], P('fs', 'tp'), may hold values from 0.05 to 1
- output_mean: float32 [256, 2048], P('fs', 'tp'), may hold values from -3 to 3
- output_square: float32 [256, 2048], P('fs', 'tp'), may hold values from 0.05 to 1
Outputs:
- step_query: float32 [512, 1536], P('fs', 'tp')
- step_output: float32 [1024, 2048], P('fs', 'tp')
- new_query: float32 [512, 1536], P('fs', 'tp')
- new_output: float32 [1024, 2048], P('fs', 'tp')
- copy_query: bfloat16 [512, 1536], P(None, 'tp')
- copy_output: bfloat16 [1024, 2048], P(None, 'tp')
- query_mean_new: float32 [256, 1536], P('fs', 'tp')
- query_square_new: float32 [256, 1536], P('fs', 'tp')
- output_mean_new: float32 [256, 2048], P('fs', 'tp')
- output_square_new: float32 [256, 2048], P('fs', 'tp')
All inputs are finite; a program needn't handle non-finite values.
Results may differ from a plain program's by a relative error of at most 0.0085.
Values may be sent and summed in bfloat16 or wider, within the bound.
A program may use at most 64 MiB of HBM per device.

v0:
```python
import math

import jax
import jax.numpy as jnp
from jax import lax
from jax.sharding import PartitionSpec as P


def sent_to_all(x, axis):
    copies = jnp.broadcast_to(x, (lax.axis_size(axis), *x.shape))
    return lax.all_to_all(copies, axis, split_axis=0, concat_axis=0, tiled=True)


def laid_out(tiles, dim):
    dims = list(tiles.shape[1:])
    dims[dim] *= tiles.shape[0]
    return jnp.moveaxis(tiles, 0, dim).reshape(dims)


def gathered_copies(x, axis, dim):
    tiles = sent_to_all(x, axis)
    return laid_out(tiles, dim)


def cut_along(x, dim, count):
    before, after = (x.shape[:dim], x.shape[dim + 1 :])
    return jnp.moveaxis(x.reshape(*before, count, -1, *after), dim, 0)


def sent_and_summed(x, axis, dim):
    tiles = cut_along(x, dim, lax.axis_size(axis))
    arrived = lax.all_to_all(tiles, axis, split_axis=0, concat_axis=0, tiled=True)
    return arrived.sum(axis=0)


def over_copies(x, axis):
    everything = sent_to_all(x, axis)
    return jnp.sum(everything, axis=0)


def in_one(arrays, axis):
    ends = [0]
    for a in arrays:
        ends.append(ends[-1] + a.size)
    subtotal = over_copies(jnp.concatenate([a.ravel() for a in arrays]), axis)
    return tuple((subtotal[b:e].reshape(a.shape) for a, b, e in zip(arrays, ends, ends[1:])))


def one_gather(arrays, axis, dims):
    vector = jnp.concatenate([a.reshape(-1) for a in arrays])
    lines, at, outs = (lax.all_gather(vector, axis), 0, [])
    for a, dim in zip(arrays, dims):
        tiles = lines[:, at : at + a.size].reshape(-1, *a.shape)
        outs.append(laid_out(tiles, dim))
        at += a.size
    return tuple(outs)


def over_rows(left, right):
    return lax.dot_general(
        left, right, (((0,), (0,)), ((), ())), preferred_element_type=jnp.float32
    )


def over_rows_exact(left, right):
    return lax.dot_general(
        left,
        right,
        (((0,), (0,)), ((), ())),
        precision=lax.Precision.HIGHEST,
        preferred_element_type=jnp.float32,
    )


def exact_dot(left, right):
    return jnp.dot(left, right, precision=lax.Precision.HIGHEST, preferred_element_type=jnp.float32)


def moments(mean, square, low):
    mean_new = 0.8 * mean + 0.2 * low
    square_new = 0.9 * square + 0.1 * low * low
    return (mean_new, square_new, mean_new / jnp.sqrt(square_new))


def on_device(
    latent_in,
    query_cot,
    attn_out,
    mix_cot,
    query_weight,
    output_weight,
    query_factor,
    output_factor,
    query_mean,
    query_square,
    output_mean,
    output_square,
):
    tokens_local = latent_in.shape[0]
    inv_root = 1.0 / math.sqrt(tokens_local * lax.axis_size("fs"))
    weight_rows = query_weight.shape[0]
    query_width = query_weight.shape[1]
    output_width = output_weight.shape[1]
    rank = query_factor.shape[1]
    factor_query = query_factor.astype(jnp.float32)
    factor_output = output_factor.astype(jnp.float32)
    stacked = jnp.concatenate([query_factor, output_factor.reshape(weight_rows, 2 * rank)], axis=1)
    whole_factors = gathered_copies(stacked, "fs", 0).astype(jnp.float32)
    all_rows = whole_factors.shape[0]
    whole_query = whole_factors[:, :rank]
    whole_output = whole_factors[:, rank:].reshape(2 * all_rows, rank)
    partial_query = over_rows(latent_in, query_cot)
    partial_output = over_rows(attn_out, mix_cot)
    low = sent_and_summed(
        jnp.concatenate(
            [
                over_rows_exact(whole_query, partial_query),
                over_rows_exact(whole_output, partial_output),
            ],
            axis=1,
        )
        * inv_root,
        "fs",
        0,
    )
    mean_q, square_q, direction_q = moments(query_mean, query_square, low[:, :query_width])
    mean_o, square_o, direction_o = moments(output_mean, output_square, low[:, query_width:])
    joined = jnp.concatenate([direction_q, direction_o], axis=1)
    piece = gathered_copies(joined, "fs", 0)
    piece_query = piece[:, :query_width]
    piece_output = piece[:, query_width:]
    product_q = exact_dot(factor_query, piece_query)
    product_o = exact_dot(factor_output, piece_output)
    square_sum_q = jnp.sum(piece_query * piece_query)
    square_sum_o = jnp.sum(piece_output * piece_output)
    square_sum_q, square_sum_o = in_one((square_sum_q, square_sum_o), "tp")
    columns = lax.axis_size("tp")
    scale_q = 1.0 / jnp.sqrt(square_sum_q / (rank * query_width * columns) + 0.25)
    scale_o = 1.0 / jnp.sqrt(square_sum_o / (rank * output_width * columns) + 0.25)
    step_q = product_q * scale_q
    step_o = product_o * scale_o
    new_q = query_weight - 0.02 * step_q
    new_o = output_weight - 0.02 * step_o
    copy_q, copy_o = one_gather(
        (new_q.astype(jnp.bfloat16), new_o.astype(jnp.bfloat16)), "fs", (0, 0)
    )
    return (step_q, step_o, new_q, new_o, copy_q, copy_o, mean_q, square_q, mean_o, square_o)


def solution(mesh):
    placed = (
        P("fs", None),
        P("fs", "tp"),
        P("fs", None),
        P("fs", "tp"),
        P("fs", "tp"),
        P("fs", "tp"),
        P("fs", None),
        P("fs", None),
        P("fs", "tp"),
        P("fs", "tp"),
        P("fs", "tp"),
        P("fs", "tp"),
    )
    return jax.shard_map(
        on_device,
        mesh=mesh,
        in_specs=placed,
        out_specs=(
            P("fs", "tp"),
            P("fs", "tp"),
            P("fs", "tp"),
            P("fs", "tp"),
            P(None, "tp"),
            P(None, "tp"),
            P("fs", "tp"),
            P("fs", "tp"),
            P("fs", "tp"),
            P("fs", "tp"),
        ),
        check_vma=False,
    )
```

profile of v0, /device:TPU:2, one launch (start us, length us, event | category | flops | bytes accessed | tf_op | source)
XLA Modules:
  0.0 175.2 jit_solution(3181078471940393403)
XLA Ops:
  0.7 0.9 reshape.64
  1.5 0.8 pad_maximum_fusion
  2.3 0.9 broadcast_in_dim.9
  3.3 11.6 %all-to-all-start = ((bf16[32,16,768]{2,1,0:T(8,128)(2,1)}), bf16[32,16,768]{2,1,0:T(8,128)(2,1)}, u32[]{:S(2)}, u32[]{:S(2)}) async-start(bf16[32,16,768]{2,1,0:T(8,128)(2,1)} %broadcast_in_dim.9), calls=%async_computation | async-start | bytes 1572864 | tf_op jit(solution)/shard_map/all_to_all | solution.py:11
  14.9 2.2 %fusion.13 = f32[512,192]{0,1:T(8,128)S(1)} fusion(bf16[3072,192]{0,1:T(8,128)(2,1)} %param.13, bf16[3072,512]{1,0:T(8,128)(2,1)S(1)} %copy-done), kind=kOutput, calls=%fused_computation.31 | convolution fusion | flops 603979776 | bytes 4718592 | tf_op jit(solution)/shard_map/dot_general | solution.py:60
  17.1 5.6 %convolution_bitcast_fusion = f32[1024,256,1]{1,0,2:T(8,128)} fusion(bf16[3072,1024]{1,0:T(8,128)(2,1)} %param.14, bf16[3072,256]{1,0:T(8,128)(2,1)S(1)} %copy-done.2), kind=kOutput, calls=%fused_computation | convolution fusion | flops 1610612736 | bytes 8912896 | tf_op jit(solution)/shard_map/dot_general | solution.py:60
  22.7 15.1 %all-to-all-done = bf16[32,16,768]{2,1,0:T(8,128)(2,1)} async-done(((bf16[32,16,768]{2,1,0:T(8,128)(2,1)}), bf16[32,16,768]{2,1,0:T(8,128)(2,1)}, u32[]{:S(2)}, u32[]{:S(2)}) %all-to-all-start) | async-done | bytes 786464 | tf_op jit(solution)/shard_map/all_to_all | solution.py:11
  37.7 1.9 %slice.41 = bf16[512,512]{1,0:T(8,128)(2,1)} slice(bf16[512,768]{1,0:T(8,128)(2,1)} %bitcast), slice={[0:512], [256:768]} | slice | bytes 1048576 | tf_op jit(solution)/shard_map/slice | solution.py:111
  39.6 2.1 %convolution_bitcast_fusion.1 = f32[32,8,192]{2,1,0:T(8,128)} fusion(f32[512,192]{0,1:T(8,128)S(1)} %fusion.13, bf16[512,768]{1,0:T(8,128)(2,1)} %bitcast), kind=kOutput, calls=%fused_computation.1 | convolution fusion | flops 301989888 | bytes 851968 | tf_op jit(solution)/shard_map/dot_general | solution.py:66
  41.7 2.1 %reshape.66 = bf16[1024,256]{1,0:T(8,128)(2,1)} reshape(bf16[512,512]{1,0:T(8,128)(2,1)} %slice.41) | data formatting | bytes 1048576 | tf_op jit(solution)/shard_map/reshape | solution.py:111
  43.8 2.0 %copy.45 = bf16[256,1024]{1,0:T(8,128)(2,1)} copy(bf16[256,1024]{0,1:T(8,128)(2,1)} %bitcast.33) | data formatting | bytes 1048576 | tf_op jit(solution)/shard_map/dot_general | solution.py:66
  45.8 2.1 %fusion.2 = f32[32,8,256]{2,1,0:T(8,128)S(1)} fusion(f32[1024,256,1]{1,0,2:T(8,128)} %convolution_bitcast_fusion, bf16[256,1024]{1,0:T(8,128)(2,1)} %copy.45), kind=kOutput, calls=%fused_computation.7 | convolution fusion | flops 805306368 | bytes 1835008 | tf_op jit(solution)/shard_map/dot_general | solution.py:66
  48.2 21.7 %all_to_all.21 = f32[32,8,448]{2,1,0:T(8,128)} all-to-all(f32[32,8,448]{2,1,0:T(8,128)S(1)} %maximum_multiply_fusion), channel_id=1, replica_groups=mesh['fs'=32,'tp'=8] {'fs'}, dimensions={0} | all-to-all | bytes 917504 | tf_op jit(solution)/shard_map/all_to_all | solution.py:32
  69.9 1.1 reduce_sum.36
  71.0 0.7 rsqrt_multiply_fusion
  71.7 0.6 rsqrt_multiply_fusion.1
  72.4 21.0 %all_to_all.22 = f32[32,8,448]{2,1,0:T(8,128)S(1)} all-to-all(f32[32,8,448]{2,1,0:T(8,128)S(1)} %broadcast_in_dim.10), channel_id=1, replica_groups=mesh['fs'=32,'tp'=8] {'fs'}, dimensions={0} | all-to-all | bytes 917504 | tf_op jit(solution)/shard_map/all_to_all | solution.py:11
  93.5 0.7 multiply_reduce_fusion
  94.3 0.8 copy.51
  95.1 1.6 multiply_reduce_fusion.1
  96.7 1.4 pad_maximum_fusion.3
  98.0 8.5 %all_to_all.23 = f32[8,1,2]{2,1,0:T(1,128)S(1)} all-to-all(f32[8,1,2]{2,1,0:T(1,128)S(1)} %broadcast_in_dim.11), channel_id=1, replica_groups=mesh['fs'=32,'tp'=8] {'tp'}, dimensions={0} | all-to-all | bytes 128 | tf_op jit(solution)/shard_map/all_to_all | solution.py:11
  108.5 1.3 fusion
  109.8 1.8 %fusion.9 = (bf16[16,192]{1,0:T(8,128)(2,1)S(1)}, f32[16,192]{1,0:T(8,128)}, f32[16,192]{1,0:T(8,128)}) fusion(f32[16,192]{1,0:T(8,128)S(1)} %copy-done.8, f32[]{:T(128)} %bitcast.8, bf16[16,256]{1,0:T(8,128)(2,1)S(1)} %copy-done.7, f32[256,448]{1,0:T(8,128)} %bitcast.32), kind=kOutput, calls=%fused_computation.29 | convolution fusion | flops 9449472 | bytes 313856 | tf_op jit(solution)/shard_map/dot_general | solution.py:76
  111.7 0.6 convert_bitcast_fusion
  112.4 53.0 %all-gather = bf16[360448]{0:T(1024)(128)(2,1)} all-gather(bf16[11264]{0:T(1024)(128)(2,1)S(1)} %pad_maximum_fusion.1), channel_id=2, replica_groups=mesh['fs'=32,'tp'=8] {'fs'}, dimensions={0}, use_global_device_ids=true | all-gather | bytes 743424 | tf_op jit(solution)/shard_map/all_gather | solution.py:51
  165.4 2.1 %reshape.72 = bf16[32,11264]{1,0:T(8,128)(2,1)} reshape(bf16[360448]{0:T(1024)(128)(2,1)} %all-gather) | data formatting | bytes 1441792 | tf_op jit(solution)/shard_map/all_gather | solution.py:51
  167.5 1.6 slice.46
  169.2 1.9 %slice.47 = bf16[32,8192]{1,0:T(8,128)(2,1)} slice(bf16[32,11264]{1,0:T(8,128)(2,1)} %reshape.72), slice={[0:32], [3072:11264]} | slice | bytes 1048576 | tf_op jit(solution)/shard_map/slice | solution.py:53
  171.0 2.1 %reshape_reshape.7 = bf16[1024,256]{1,0:T(8,128)(2,1)} reshape(bf16[32,8192]{1,0:T(8,128)(2,1)} %slice.47) | data formatting | bytes 1048576 | tf_op jit(solution)/shard_map/reshape;reshape | solution.py:17
  173.1 1.2 reshape_reshape.6
  174.4 0.8 copy.48
  (36 shorter events, 1.2 us)
Async XLA Ops:
  0.6 14.2 %copy-start = (bf16[3072,512]{1,0:T(8,128)(2,1)S(1)}, bf16[3072,512]{1,0:T(8,128)(2,1)}, u32[]{:S(2)}) copy-start(bf16[3072,512]{1,0:T(8,128)(2,1)} %param.12) | copy-start | bytes 9437188
  3.3 34.5 %all-to-all-start = ((bf16[32,16,768]{2,1,0:T(8,128)(2,1)}), bf16[32,16,768]{2,1,0:T(8,128)(2,1)}, u32[]{:S(2)}, u32[]{:S(2)}) async-start(bf16[32,16,768]{2,1,0:T(8,128)(2,1)} %broadcast_in_dim.9), calls=%async_computation | async-start | bytes 1572864 | tf_op jit(solution)/shard_map/all_to_all | solution.py:11
  14.9 2.2 %copy-start.2 = (bf16[3072,256]{1,0:T(8,128)(2,1)S(1)}, bf16[3072,256]{1,0:T(8,128)(2,1)}, u32[]{:S(2)}) copy-start(bf16[3072,256]{1,0:T(8,128)(2,1)} %param.15) | copy-start | bytes 4718596
  41.7 6.2 %copy-start.3 = (f32[32,8,192]{2,1,0:T(8,128)S(1)}, f32[32,8,192]{2,1,0:T(8,128)}, u32[]{:S(2)}) copy-start(f32[32,8,192]{2,1,0:T(8,128)} %convolution_bitcast_fusion.1) | copy-start | bytes 589828
  41.7 29.3 %copy-start.9 = (f32[8,256]{1,0:T(8,128)S(1)}, f32[8,256]{1,0:T(8,128)}, u32[]{:S(2)}) copy-start(f32[8,256]{1,0:T(8,128)} %param.23) | copy-start | bytes 24580
  41.7 29.3 %copy-start.10 = (f32[8,256]{1,0:T(8,128)S(1)}, f32[8,256]{1,0:T(8,128)}, u32[]{:S(2)}) copy-start(f32[8,256]{1,0:T(8,128)} %param.22) | copy-start | bytes 24580
  41.7 30.0 %copy-start.11 = (f32[8,192]{1,0:T(8,128)S(1)}, f32[8,192]{1,0:T(8,128)}, u32[]{:S(2)}) copy-start(f32[8,192]{1,0:T(8,128)} %param.21) | copy-start | bytes 18436
  41.7 30.0 %copy-start.12 = (f32[8,192]{1,0:T(8,128)S(1)}, f32[8,192]{1,0:T(8,128)}, u32[]{:S(2)}) copy-start(f32[8,192]{1,0:T(8,128)} %param.20) | copy-start | bytes 18436
  47.9 60.6 %copy-start.5 = (bf16[32,256]{1,0:T(8,128)(2,1)S(1)}, bf16[32,256]{1,0:T(8,128)(2,1)}, u32[]{:S(2)}) copy-start(bf16[32,256]{1,0:T(8,128)(2,1)} %param.19) | copy-start | bytes 49156
  47.9 61.9 %copy-start.7 = (bf16[16,256]{1,0:T(8,128)(2,1)S(1)}, bf16[16,256]{1,0:T(8,128)(2,1)}, u32[]{:S(2)}) copy-start(bf16[16,256]{1,0:T(8,128)(2,1)} %param.18) | copy-start | bytes 24580
  48.0 61.9 %copy-start.8 = (f32[16,192]{1,0:T(8,128)S(1)}, f32[16,192]{1,0:T(8,128)}, u32[]{:S(2)}) copy-start(f32[16,192]{1,0:T(8,128)} %param.16) | copy-start | bytes 36868
  48.0 63.8 %copy-start.6 = (f32[32,256]{1,0:T(8,128)S(1)}, f32[32,256]{1,0:T(8,128)}, u32[]{:S(2)}) copy-start(f32[32,256]{1,0:T(8,128)} %param.17) | copy-start | bytes 98308
  93.5 0.8 copy-start.1
  109.8 65.3 %copy-start.4 = (f32[32,256]{1,0:T(8,128)}, f32[32,256]{1,0:T(8,128)S(1)}, u32[]{:S(2)}) copy-start(f32[32,256]{1,0:T(8,128)S(1)} %fusion) | copy-start | bytes 98308
where the time goes:
time: 176 us; the launch traced here: 175 us
  blocking collectives  104 us (59%)
  local copies, waits for them, and re-layouts  19.2 us (11%)
  matrix products  15.1 us (9%)
  waiting for transfers between devices  15.1 us (9%)
  starting transfers between devices  11.6 us (7%)
  other arithmetic  7.72 us (4%)
  between operations  2.24 us (1%)
    all_gather x1, blocking collectives, one_gather(): lines, at, outs = (lax.all_gather(vector, axis), 0, [])  53 us
    all_to_all x2, blocking collectives, sent_to_all(): return lax.all_to_all(copies, axis, split_axis=0, concat_axis=0, tiled=True)  29.5 us
    all_to_all x1, blocking collectives, sent_and_summed(): lax.all_to_all(tiles, axis, split_axis=0, concat_axis=0, tiled=True)  21.7 us
    all_to_all x1, waiting for transfers between devices, sent_to_all(): return lax.all_to_all(copies, axis, split_axis=0, concat_axis=0, tiled=True)  15.1 us
    all_to_all x1, starting transfers between devices, sent_to_all(): return lax.all_to_all(copies, axis, split_axis=0, concat_axis=0, tiled=True)  11.6 us
    dot_general x2, matrix products, over_rows(): lax.dot_general(left, right, (((0,), (0,)), ((), ())), preferred_element_...  7.78 us
    dot_general x2, matrix products, over_rows_exact(): lax.dot_general(left, right, (((0,), (0,)), ((), ())), precision=lax.Prec...  4.18 us
  transfers between devices with their start and end apart: 1, of which 1 were waited for; matrix products, arithmetic and copies ran while one was open for 4% of the time, Pallas kernels for 0%

commit v1 on v0

v1 whole, which is shorter than its diff:
```python
import functools
import math

import jax
import jax.numpy as jnp
from jax import lax
from jax.experimental import pallas as pl
from jax.experimental.pallas import tpu as pltpu
from jax.sharding import PartitionSpec as P

MESH = pl.DeviceIdType.MESH
F32 = jnp.float32
BF16 = jnp.bfloat16
NZ, NY = 8, 4
CHUNKS = 6
Z_ORDER = (1, 7, 2, 6, 3, 5, 4)
FAR_FIRST = (4, 3, 5, 2, 6, 1, 7)
FORWARD_UP = (0, 7, 6, 5)
FORWARD_DOWN = (1, 2, 3, 4)


def by_tokens(left, right):
    return lax.dot_general(left, right, (((0,), (0,)), ((), ())), preferred_element_type=F32)


def dot(left, right):
    return jnp.dot(left, right, preferred_element_type=F32)


def split_dot(left, right):
    high = left.astype(BF16)
    low = (left - high.astype(F32)).astype(BF16)
    return dot(high, right) + dot(low, right)


def kernel(
    inv_root,
    lat, qcot, att, mix, qw, ow, qf, of, qm, qs, om, os_,
    step_q, step_o, new_q, new_o, copy_q, copy_o, mean_q, square_q, mean_o, square_o,
    lat_v, qcot_v, att_v, mix_v, qw_v, ow_v, qm_v, qs_v, om_v, os_v,
    gq, go, fac, wei, part, part_in, mid, mid_in, drc, sums, sums_in,
    pq, po, cq, co, sq_v, so_v, nq_v, no_v, mq_v, sqq_v, mo_v, soo_v,
    chunk_sem, small_sem, out_sem,
    fz_s, fz_r, fy_s, fy_r, fw_s, fw_r, fd_s, fd_r,
    wz_s, wz_r, wy_s, wy_r, ww_s, ww_r,
    py_s, py_r, pz_s, pz_r,
    dz_s, dz_r, dy_s, dy_r, dw_s, dw_r,
    st_s, st_r, sy_s, sy_r,
):
    fs, tp = lax.axis_index("fs"), lax.axis_index("tp")
    y, z = lax.rem(fs, NY), fs // NY
    core = lax.rem(tp, 2)
    other = 1 - core
    partner = (fs, tp + 1 - 2 * core)
    ups = [lax.rem(y + d, NY) for d in range(NY)]
    downs = [lax.rem(y + NY - d, NY) for d in range(NY)]
    zup = [lax.rem(z + d, NZ) for d in range(NZ)]
    zdn = [lax.rem(z + NZ - d, NZ) for d in range(NZ)]

    def at_y(row):
        return (z * NY + row, tp)

    def at_z(level):
        return (level * NY + y, tp)

    def at_tp(d):
        return (fs, lax.rem(tp + d, 8))

    def remote(src, dst, send, recv, to):
        return pltpu.make_async_remote_copy(
            src_ref=src, dst_ref=dst, send_sem=send, recv_sem=recv, device_id=to, device_id_type=MESH
        )

    barrier = pltpu.get_barrier_semaphore()
    for to in [at_y(ups[d]) for d in range(1, NY)] + [at_z(zup[d]) for d in range(1, NZ)] + [at_tp(d) for d in range(1, 8)]:
        pl.semaphore_signal(barrier, inc=1, device_id=to, device_id_type=MESH)

    half = pl.ds(pl.multiple_of(core * 128, 128), 128)
    own = fac.at[core, z, y]
    small = []
    for i, (src, dst) in enumerate((
        (qf.at[:, half], own.at[pl.ds(0, 16)]),
        (of.at[:, half], own.at[pl.ds(16, 32)]),
        (qw, qw_v), (ow, ow_v), (qm, qm_v), (qs, qs_v), (om, om_v), (os_, os_v),
    )):
        small.append(pltpu.make_async_copy(src, dst, small_sem.at[i]))
        small[-1].start()

    tokens = lat.shape[0]
    rows = tokens // CHUNKS
    pairs = ((qcot, qcot_v), (lat, lat_v), (mix, mix_v), (att, att_v))

    def chunk_copies(i):
        span = pl.ds(pl.multiple_of(i * rows, rows), rows)
        return [
            pltpu.make_async_copy(src.at[span], dst.at[span], chunk_sem.at[i, j])
            for j, (src, dst) in enumerate(pairs)
        ]

    for i in range(CHUNKS):
        for copy in chunk_copies(i):
            copy.start()

    gq[...] = jnp.zeros_like(gq)
    go[...] = jnp.zeros_like(go)

    def add_chunk(i):
        for copy in chunk_copies(i):
            copy.wait()
        span = pl.ds(pl.multiple_of(i * rows, rows), rows)
        gq[...] += by_tokens(qcot_v[span, :], lat_v[span, :])
        go[...] += by_tokens(mix_v[span, :], att_v[span, :])

    def add_chunks(a, b):
        @pl.loop(a, b)
        def _(i):
            add_chunk(i)

    for copy in small:
        copy.wait()
    qcols = qw_v.shape[1]
    wei[z, y, 0:16, 0:qcols] = qw_v[...].astype(BF16)
    wei[z, y, 16:48, :] = ow_v[...].astype(BF16)

    add_chunks(0, 1)
    pl.semaphore_wait(barrier, 17)

    def f_blk(level, row):
        return fac.at[core, level, row]

    def w_blk(level, row):
        return wei.at[level, row]

    def d_blk(level, row):
        return drc.at[level, row]

    started = []

    def start(copy):
        copy.start()
        started.append(copy)

    def z_send(blk, s, r):
        for k in FAR_FIRST:
            start(remote(blk(z, y), blk(z, y), s.at[k], r.at[k], at_z(zup[k])))

    def z_wait(blk, s, r, k):
        remote(blk(zdn[k], y), blk(zdn[k], y), s.at[k], r.at[k], at_z(zup[k])).wait_recv()

    def y_send(blk, s, r, k):
        for way, row in ((0, ups[1]), (1, downs[1])):
            start(remote(blk(zdn[k], y), blk(zdn[k], y), s.at[way, k], r.at[way, k], at_y(row)))

    def y_wait(blk, s, r, way, k):
        row = downs[1] if way == 0 else ups[1]
        remote(blk(zdn[k], row), blk(zdn[k], row), s.at[way, k], r.at[way, k], at_y(row)).wait_recv()

    def w_send(blk, s, r, k):
        if k in FORWARD_UP:
            src, to = blk(zdn[k], downs[1]), ups[1]
        else:
            src, to = blk(zdn[k], ups[1]), downs[1]
        start(remote(src, src, s.at[k], r.at[k], at_y(to)))

    def w_wait(blk, s, r, k):
        dst = blk(zdn[k], ups[2])
        remote(dst, dst, s.at[k], r.at[k], at_y(ups[1])).wait_recv()

    def swap_send(row, i):
        src = fac.at[core, :, row]
        start(remote(src, src, fd_s.at[i], fd_r.at[i], partner))

    def swap_wait(row, i):
        dst = fac.at[other, :, row]
        remote(dst, dst, fd_s.at[i], fd_r.at[i], partner).wait_recv()

    z_send(f_blk, fz_s, fz_r)
    y_send(f_blk, fy_s, fy_r, 0)
    z_send(w_blk, wz_s, wz_r)
    add_chunks(1, 3)
    for k in Z_ORDER[:4]:
        z_wait(f_blk, fz_s, fz_r, k)
        y_send(f_blk, fy_s, fy_r, k)
    add_chunks(3, 4)
    for k in Z_ORDER[4:]:
        z_wait(f_blk, fz_s, fz_r, k)
        y_send(f_blk, fy_s, fy_r, k)
    swap_send(y, 0)
    order = (0,) + Z_ORDER
    for k in order[:4]:
        for way in (0, 1):
            y_wait(f_blk, fy_s, fy_r, way, k)
        w_send(f_blk, fw_s, fw_r, k)
    add_chunks(4, CHUNKS)
    for k in order[4:]:
        for way in (0, 1):
            y_wait(f_blk, fy_s, fy_r, way, k)
        w_send(f_blk, fw_s, fw_r, k)
    swap_send(downs[1], 1)
    swap_send(ups[1], 2)
    for k in order:
        w_wait(f_blk, fw_s, fw_r, k)
    swap_send(ups[2], 3)
    for i, row in enumerate((y, ups[1], downs[1], ups[2])):
        swap_wait(row, i)

    def factor(first, count):
        return jnp.concatenate(
            [fac[c, :, :, first:first + count, :].reshape(32 * count, 128) for c in (0, 1)], axis=1
        )

    low_q = split_dot(gq[...], factor(0, 16)) * inv_root
    low_q = jnp.concatenate([low_q, jnp.zeros((256 - qcols, 256), F32)], axis=0).T
    low_o = (split_dot(go[...], factor(16, 32)) * inv_root).T
    for row in range(NY):
        part[row] = jnp.concatenate(
            [low_q.reshape(NZ, NY, 8, 256)[:, row], low_o.reshape(NZ, NY, 8, 256)[:, row]], axis=1
        ).astype(BF16)

    for d in (2, 1, 3):
        start(remote(part.at[ups[d]], part_in.at[d], py_s.at[d], py_r.at[d], at_y(ups[d])))
    for k in Z_ORDER:
        z_wait(w_blk, wz_s, wz_r, k)
    for way, row in ((0, ups[1]), (1, downs[1])):
        src = wei.at[:, y]
        start(remote(src, src, wy_s.at[way], wy_r.at[way], at_y(row)))
    total = part[y].astype(F32)
    for d in (1, 3, 2):
        remote(part.at[y], part_in.at[d], py_s.at[d], py_r.at[d], at_y(ups[d])).wait_recv()
        total = total + part_in[d].astype(F32)
    mid[...] = total.astype(BF16)
    for k in FAR_FIRST:
        start(remote(mid.at[zup[k]], mid_in.at[k], pz_s.at[k], pz_r.at[k], at_z(zup[k])))
    low = mid[z].astype(F32)
    for k in Z_ORDER:
        remote(mid.at[z], mid_in.at[k], pz_s.at[k], pz_r.at[k], at_z(zup[k])).wait_recv()
        low = low + mid_in[k].astype(F32)

    def moments(mean, square, low):
        mean_new = 0.8 * mean + 0.2 * low
        square_new = 0.9 * square + 0.1 * low * low
        return (mean_new, square_new, mean_new / jnp.sqrt(square_new))

    mq_v[...], sqq_v[...], dir_q = moments(qm_v[...], qs_v[...], low[0:8, 0:qcols])
    mo_v[...], soo_v[...], dir_o = moments(om_v[...], os_v[...], low[8:16, :])
    dir_q = jnp.concatenate([dir_q, jnp.zeros((8, 256 - qcols), F32)], axis=1)
    drc[z, y] = jnp.concatenate([dir_q, dir_o], axis=0).astype(BF16)
    z_send(d_blk, dz_s, dz_r)
    y_send(d_blk, dy_s, dy_r, 0)

    outs = []

    def put(src, dst):
        outs.append(pltpu.make_async_copy(src, dst, out_sem.at[len(outs)]))
        outs[-1].start()

    put(mq_v, mean_q)
    put(sqq_v, square_q)
    put(mo_v, mean_o)
    put(soo_v, square_o)

    for k in Z_ORDER:
        z_wait(d_blk, dz_s, dz_r, k)
        y_send(d_blk, dy_s, dy_r, k)
    column = drc[:, y].astype(F32)
    square = column * column
    sum_q = jnp.sum(square[:, 0:8].reshape(64, 256), axis=(0, 1), keepdims=True)
    sum_o = jnp.sum(square[:, 8:16].reshape(64, 256), axis=(0, 1), keepdims=True)
    sums[0] = jnp.concatenate([jnp.broadcast_to(sum_q, (4, 128)), jnp.broadcast_to(sum_o, (4, 128))], axis=0)
    for d in range(1, 8):
        start(remote(sums.at[0], sums_in.at[d], st_s.at[d], st_r.at[d], at_tp(d)))

    for k in order:
        for way in (0, 1):
            y_wait(d_blk, dy_s, dy_r, way, k)
        w_send(d_blk, dw_s, dw_r, k)
    for way in (0, 1):
        row = downs[1] if way == 0 else ups[1]
        src = wei.at[:, row]
        remote(src, src, wy_s.at[way], wy_r.at[way], at_y(row)).wait_recv()
    for i, (lo, row, to) in enumerate(((0, downs[1], ups[1]), (4, ups[1], downs[1]))):
        src = wei.at[pl.ds(lo, 4), row]
        start(remote(src, src, ww_s.at[i], ww_r.at[i], at_y(to)))

    total = sums[0]
    for d in range(1, 8):
        remote(sums.at[0], sums_in.at[d], st_s.at[d], st_r.at[d], at_tp(d)).wait_recv()
        total = total + sums_in[d]
    sums[1] = total
    for d in (1, 2, 3):
        start(remote(sums.at[1], sums_in.at[7 + d], sy_s.at[d], sy_r.at[d], at_y(ups[d])))

    for k in order:
        w_wait(d_blk, dw_s, dw_r, k)
    every = drc[...].astype(F32).reshape(32, 16, 256)
    pq[...] = dot(factor(0, 16), every[:, 0:8].reshape(256, 256).astype(BF16))
    po[...] = dot(factor(16, 32), every[:, 8:16].reshape(256, 256).astype(BF16))
    for d in (1, 2, 3):
        remote(sums.at[1], sums_in.at[7 + d], sy_s.at[d], sy_r.at[d], at_y(ups[d])).wait_recv()
        total = total + sums_in[7 + d]
    count = 256.0 * 8 * qcols
    scale_q = lax.rsqrt(total[0:1, 0:1] / count + 0.25)
    scale_o = lax.rsqrt(total[4:5, 0:1] / (256.0 * 8 * 256) + 0.25)

    own_q = pq[pl.ds(pl.multiple_of(fs * 16, 16), 16), :][:, 0:qcols] * scale_q
    own_o = po[pl.ds(pl.multiple_of(fs * 32, 32), 32), :] * scale_o
    sq_v[...] = own_q
    so_v[...] = own_o
    nq_v[...] = qw_v[...] - 0.02 * own_q
    no_v[...] = ow_v[...] - 0.02 * own_o
    put(sq_v, step_q)
    put(so_v, step_o)
    put(nq_v, new_q)
    put(no_v, new_o)
    for i in (0, 1):
        dst = wei.at[pl.ds(4 * i, 4), ups[2]]
        remote(dst, dst, ww_s.at[i], ww_r.at[i], at_y(ups[1])).wait_recv()
    weights = wei[...].reshape(32, 48, 256).astype(F32)
    weights_q = weights[:, 0:16].reshape(512, 256)
    weights_o = weights[:, 16:48].reshape(1024, 256)
    cq[...] = (weights_q - 0.02 * (pq[...] * scale_q))[:, 0:qcols].astype(BF16)
    put(cq, copy_q)
    co[...] = (weights_o - 0.02 * (po[...] * scale_o)).astype(BF16)
    put(co, copy_o)
    for copy in started:
        copy.wait_send()
    for copy in outs:
        copy.wait()


def solution(mesh):
    def on_device(lat, qcot, att, mix, qw, ow, qf, of, qm, qs, om, os_):
        tokens, qcols = lat.shape[0], qw.shape[1]
        inv_root = 1.0 / math.sqrt(tokens * lax.axis_size("fs"))

        def like(a):
            return jax.ShapeDtypeStruct(a.shape, a.dtype)

        def vm(a):
            return pltpu.VMEM(a.shape, a.dtype)

        dma = pltpu.SemaphoreType.DMA
        any_ = pl.BlockSpec(memory_space=pl.ANY)
        outs = (
            like(qw), like(ow), like(qw), like(ow),
            jax.ShapeDtypeStruct((512, qcols), BF16), jax.ShapeDtypeStruct((1024, 256), BF16),
            like(qm), like(qs), like(om), like(os_),
        )
        return pl.pallas_call(
            functools.partial(kernel, inv_root),
            out_shape=outs,
            in_specs=[any_] * 12,
            out_specs=[any_] * 10,
            scratch_shapes=[
                vm(lat), vm(qcot), vm(att), vm(mix), vm(qw), vm(ow), vm(qm), vm(qs), vm(om), vm(os_),
                pltpu.VMEM((qcols, 512), F32), pltpu.VMEM((256, 1024), F32),
                pltpu.VMEM((2, NZ, NY, 48, 128), BF16), pltpu.VMEM((NZ, NY, 48, 256), BF16),
                pltpu.VMEM((NY, NZ, 16, 256), BF16), pltpu.VMEM((NY, NZ, 16, 256), BF16),
                pltpu.VMEM((NZ, 16, 256), BF16), pltpu.VMEM((NZ, 16, 256), BF16),
                pltpu.VMEM((NZ, NY, 16, 256), BF16),
                pltpu.VMEM((2, 8, 128), F32), pltpu.VMEM((11, 8, 128), F32),
                pltpu.VMEM((512, 256), F32), pltpu.VMEM((1024, 256), F32),
                pltpu.VMEM((512, qcols), BF16), pltpu.VMEM((1024, 256), BF16),
                vm(qw), vm(ow), vm(qw), vm(ow), vm(qm), vm(qs), vm(om), vm(os_),
                dma((CHUNKS, 4)), dma((8,)), dma((10,)),
                dma((8,)), dma((8,)), dma((2, 8)), dma((2, 8)), dma((8,)), dma((8,)), dma((4,)), dma((4,)),
                dma((8,)), dma((8,)), dma((2,)), dma((2,)), dma((2,)), dma((2,)),
                dma((4,)), dma((4,)), dma((8,)), dma((8,)),
                dma((8,)), dma((8,)), dma((2, 8)), dma((2, 8)), dma((8,)), dma((8,)),
                dma((8,)), dma((8,)), dma((4,)), dma((4,)),
            ],
            compiler_params=pltpu.CompilerParams(
                collective_id=0, has_side_effects=True, vmem_limit_bytes=56 * 1024 * 1024
            ),
        )(lat, qcot, att, mix, qw, ow, qf, of, qm, qs, om, os_)

    rows, both, whole = P("fs", None), P("fs", "tp"), P(None, "tp")
    return jax.shard_map(
        on_device,
        mesh=mesh,
        in_specs=(rows, both, rows, both, both, both, rows, rows, both, both, both, both),
        out_specs=(both, both, both, both, whole, whole, both, both, both, both),
        check_vma=False,
    )
```

time: 176 us -> 66.8 us (0.38)
  the two profiles are of different devices: /device:TPU:2 before, /device:TPU:1 now
where the time goes in v1:
time: 66.8 us; the launch traced here: 66.4 us
  Pallas kernels  51.7 us (77%)
  local copies, waits for them, and re-layouts  14 us (21%)
  between operations  0.69 us (1%)
    pallas_call x1, Pallas kernels, on_device(): pl.pallas_call(functools.partial(kernel, inv_root), out_shape=outs, in_sp...  51.7 us
    unnamed x18, local copies, waits for them, and re-layouts  12.2 us
    pallas_call x1, local copies, waits for them, and re-layouts, on_device(): pl.pallas_call(functools.partial(kernel, inv_root), out_shape=outs, in_sp...  1.78 us

profile of v1, /device:TPU:1, one launch (start us, length us, event | category | flops | bytes accessed | tf_op | source)
XLA Modules:
  0.0 66.4 jit_solution(2630887235049551446)
XLA Ops:
  0.6 2.5 %copy.22.qcot = bf16[3072,192]{1,0:T(8,128)(2,1)} copy(bf16[3072,192]{0,1:T(8,128)(2,1)} %param.13) | data formatting | bytes 2359296 | tf_op args[1]
  3.2 51.7 %shard_map.195 = (f32[16,192]{1,0:T(8,128)}, f32[32,256]{1,0:T(8,128)}, f32[16,192]{1,0:T(8,128)}, f32[32,256]{1,0:T(8,128)}, bf16[512,192]{1,0:T(8,128)(2,1)}, ...) custom-call(bf16[3072,512]{1,0:T(8,128)(2,1)} %lat.1, ...), custom_call_target="tpu_custom_call" | custom-call | tf_op jit(solution)/shard_map/pallas_call | solution.py:349
  54.9 0.0 copy-start.3
  54.9 0.0 copy-start.2
  54.9 0.0 copy-start.1
  54.9 0.0 copy-start
  54.9 1.8 %copy.23 = bf16[512,192]{0,1:T(8,128)(2,1)} copy(bf16[512,192]{1,0:T(8,128)(2,1)} %get-tuple-element.14) | data formatting | bytes 393216 | tf_op jit(solution)/shard_map/pallas_call | solution.py:349
  56.7 1.3 %copy.33 = f32[16,192]{1,0:T(8,128)} copy(f32[16,192]{1,0:T(8,128)} %get-tuple-element.30) | data formatting | bytes 24576
  58.0 1.4 %copy.34 = f32[32,256]{1,0:T(8,128)} copy(f32[32,256]{1,0:T(8,128)} %get-tuple-element.31) | data formatting | bytes 65536
  59.4 1.3 %copy.35 = f32[16,192]{1,0:T(8,128)} copy(f32[16,192]{1,0:T(8,128)} %get-tuple-element.32) | data formatting | bytes 24576
  60.7 1.4 %copy.36 = f32[32,256]{1,0:T(8,128)} copy(f32[32,256]{1,0:T(8,128)} %get-tuple-element.33) | data formatting | bytes 65536
  62.1 1.9 %copy.37 = bf16[1024,256]{1,0:T(8,128)(2,1)} copy(bf16[1024,256]{1,0:T(8,128)(2,1)} %get-tuple-element.35) | data formatting | bytes 1048576
  64.0 0.0 copy-done.3
  64.0 0.6 copy.38
  64.6 0.0 copy-done.2
  64.6 0.6 copy.39
  65.2 0.0 copy-done.1
  65.2 0.6 copy.40
  65.8 0.0 copy-done
  65.8 0.6 copy.41
Async XLA Ops:
  54.9 9.1 %copy-start.3 = (f32[8,192]{1,0:T(8,128)S(1)}, f32[8,192]{1,0:T(8,128)}, u32[]{:S(2)}) copy-start(f32[8,192]{1,0:T(8,128)} %get-tuple-element.36) | copy-start | bytes 18436
  54.9 9.7 %copy-start.2 = (f32[8,192]{1,0:T(8,128)S(1)}, f32[8,192]{1,0:T(8,128)}, u32[]{:S(2)}) copy-start(f32[8,192]{1,0:T(8,128)} %get-tuple-element.37) | copy-start | bytes 18436
  54.9 10.3 %copy-start.1 = (f32[8,256]{1,0:T(8,128)S(1)}, f32[8,256]{1,0:T(8,128)}, u32[]{:S(2)}) copy-start(f32[8,256]{1,0:T(8,128)} %get-tuple-element.38) | copy-start | bytes 24580
  54.9 10.9 %copy-start = (f32[8,256]{1,0:T(8,128)S(1)}, f32[8,256]{1,0:T(8,128)}, u32[]{:S(2)}) copy-start(f32[8,256]{1,0:T(8,128)} %get-tuple-element.39) | copy-start | bytes 24580

commit v2 on v1

--- a/solution.py
+++ b/solution.py
@@ -36,16 +36,16 @@
 def kernel(
     inv_root,
     lat, qcot, att, mix, qw, ow, qf, of, qm, qs, om, os_,
-    step_q, step_o, new_q, new_o, copy_q, copy_o, mean_q, square_q, mean_o, square_o,
+    sq_v, so_v, nq_v, no_v, cq, co, mq_v, sqq_v, mo_v, soo_v,
     lat_v, qcot_v, att_v, mix_v, qw_v, ow_v, qm_v, qs_v, om_v, os_v,
     gq, go, fac, wei, part, part_in, mid, mid_in, drc, sums, sums_in,
-    pq, po, cq, co, sq_v, so_v, nq_v, no_v, mq_v, sqq_v, mo_v, soo_v,
-    chunk_sem, small_sem, out_sem,
+    pq, po,
+    chunk_sem, small_sem,
     fz_s, fz_r, fy_s, fy_r, fw_s, fw_r, fd_s, fd_r,
     wz_s, wz_r, wy_s, wy_r, ww_s, ww_r,
     py_s, py_r, pz_s, pz_r,
     dz_s, dz_r, dy_s, dy_r, dw_s, dw_r,
-    st_s, st_r, sy_s, sy_r,
+    st_s, st_r, sz_s, sz_r, sy_s, sy_r,
 ):
     fs, tp = lax.axis_index("fs"), lax.axis_index("tp")
     y, z = lax.rem(fs, NY), fs // NY
@@ -88,18 +88,16 @@
 
     tokens = lat.shape[0]
     rows = tokens // CHUNKS
-    pairs = ((qcot, qcot_v), (lat, lat_v), (mix, mix_v), (att, att_v))
+    pairs = ((lat, lat_v), (mix, mix_v), (att, att_v))
 
     def chunk_copies(i):
         span = pl.ds(pl.multiple_of(i * rows, rows), rows)
-        return [
+        copies = [
             pltpu.make_async_copy(src.at[span], dst.at[span], chunk_sem.at[i, j])
             for j, (src, dst) in enumerate(pairs)
         ]
-
-    for i in range(CHUNKS):
-        for copy in chunk_copies(i):
-            copy.start()
+        copies.append(pltpu.make_async_copy(qcot.at[:, span], qcot_v.at[:, span], chunk_sem.at[i, 3]))
+        return copies
 
     gq[...] = jnp.zeros_like(gq)
     go[...] = jnp.zeros_like(go)
@@ -108,7 +106,7 @@
         for copy in chunk_copies(i):
             copy.wait()
         span = pl.ds(pl.multiple_of(i * rows, rows), rows)
-        gq[...] += by_tokens(qcot_v[span, :], lat_v[span, :])
+        gq[...] += dot(qcot_v[:, span], lat_v[span, :])
         go[...] += by_tokens(mix_v[span, :], att_v[span, :])
 
     def add_chunks(a, b):
@@ -118,11 +116,14 @@
 
     for copy in small:
         copy.wait()
+    for i in range(CHUNKS):
+        for copy in chunk_copies(i):
+            copy.start()
     qcols = qw_v.shape[1]
     wei[z, y, 0:16, 0:qcols] = qw_v[...].astype(BF16)
     wei[z, y, 16:48, :] = ow_v[...].astype(BF16)
 
-    add_chunks(0, 1)
+    add_chunks(0, 2)
     pl.semaphore_wait(barrier, 17)
 
     def f_blk(level, row):
@@ -176,12 +177,11 @@
 
     z_send(f_blk, fz_s, fz_r)
     y_send(f_blk, fy_s, fy_r, 0)
-    z_send(w_blk, wz_s, wz_r)
-    add_chunks(1, 3)
+    add_chunks(2, 4)
     for k in Z_ORDER[:4]:
         z_wait(f_blk, fz_s, fz_r, k)
         y_send(f_blk, fy_s, fy_r, k)
-    add_chunks(3, 4)
+    add_chunks(4, CHUNKS)
     for k in Z_ORDER[4:]:
         z_wait(f_blk, fz_s, fz_r, k)
         y_send(f_blk, fy_s, fy_r, k)
@@ -191,13 +191,13 @@
         for way in (0, 1):
             y_wait(f_blk, fy_s, fy_r, way, k)
         w_send(f_blk, fw_s, fw_r, k)
-    add_chunks(4, CHUNKS)
     for k in order[4:]:
         for way in (0, 1):
             y_wait(f_blk, fy_s, fy_r, way, k)
         w_send(f_blk, fw_s, fw_r, k)
     swap_send(downs[1], 1)
     swap_send(ups[1], 2)
+    z_send(w_blk, wz_s, wz_r)
     for k in order:
         w_wait(f_blk, fw_s, fw_r, k)
     swap_send(ups[2], 3)
@@ -219,11 +219,6 @@
 
     for d in (2, 1, 3):
         start(remote(part.at[ups[d]], part_in.at[d], py_s.at[d], py_r.at[d], at_y(ups[d])))
-    for k in Z_ORDER:
-        z_wait(w_blk, wz_s, wz_r, k)
-    for way, row in ((0, ups[1]), (1, downs[1])):
-        src = wei.at[:, y]
-        start(remote(src, src, wy_s.at[way], wy_r.at[way], at_y(row)))
     total = part[y].astype(F32)
     for d in (1, 3, 2):
         remote(part.at[y], part_in.at[d], py_s.at[d], py_r.at[d], at_y(ups[d])).wait_recv()
@@ -231,6 +226,11 @@
     mid[...] = total.astype(BF16)
     for k in FAR_FIRST:
         start(remote(mid.at[zup[k]], mid_in.at[k], pz_s.at[k], pz_r.at[k], at_z(zup[k])))
+    for k in Z_ORDER:
+        z_wait(w_blk, wz_s, wz_r, k)
+    for way, row in ((0, ups[1]), (1, downs[1])):
+        src = wei.at[:, y]
+        start(remote(src, src, wy_s.at[way], wy_r.at[way], at_y(row)))
     low = mid[z].astype(F32)
     for k in Z_ORDER:
         remote(mid.at[z], mid_in.at[k], pz_s.at[k], pz_r.at[k], at_z(zup[k])).wait_recv()
@@ -248,32 +248,11 @@
     z_send(d_blk, dz_s, dz_r)
     y_send(d_blk, dy_s, dy_r, 0)
 
-    outs = []
-
-    def put(src, dst):
-        outs.append(pltpu.make_async_copy(src, dst, out_sem.at[len(outs)]))
-        outs[-1].start()
-
-    put(mq_v, mean_q)
-    put(sqq_v, square_q)
-    put(mo_v, mean_o)
-    put(soo_v, square_o)
-
-    for k in Z_ORDER:
-        z_wait(d_blk, dz_s, dz_r, k)
-        y_send(d_blk, dy_s, dy_r, k)
-    column = drc[:, y].astype(F32)
-    square = column * column
-    sum_q = jnp.sum(square[:, 0:8].reshape(64, 256), axis=(0, 1), keepdims=True)
-    sum_o = jnp.sum(square[:, 8:16].reshape(64, 256), axis=(0, 1), keepdims=True)
+    sum_q = jnp.sum(dir_q * dir_q, axis=(0, 1), keepdims=True)
+    sum_o = jnp.sum(dir_o * dir_o, axis=(0, 1), keepdims=True)
     sums[0] = jnp.concatenate([jnp.broadcast_to(sum_q, (4, 128)), jnp.broadcast_to(sum_o, (4, 128))], axis=0)
     for d in range(1, 8):
         start(remote(sums.at[0], sums_in.at[d], st_s.at[d], st_r.at[d], at_tp(d)))
-
-    for k in order:
-        for way in (0, 1):
-            y_wait(d_blk, dy_s, dy_r, way, k)
-        w_send(d_blk, dw_s, dw_r, k)
     for way in (0, 1):
         row = downs[1] if way == 0 else ups[1]
         src = wei.at[:, row]
@@ -282,22 +261,37 @@
         src = wei.at[pl.ds(lo, 4), row]
         start(remote(src, src, ww_s.at[i], ww_r.at[i], at_y(to)))
 
+    for k in Z_ORDER[:4]:
+        z_wait(d_blk, dz_s, dz_r, k)
+        y_send(d_blk, dy_s, dy_r, k)
     total = sums[0]
     for d in range(1, 8):
         remote(sums.at[0], sums_in.at[d], st_s.at[d], st_r.at[d], at_tp(d)).wait_recv()
         total = total + sums_in[d]
     sums[1] = total
-    for d in (1, 2, 3):
-        start(remote(sums.at[1], sums_in.at[7 + d], sy_s.at[d], sy_r.at[d], at_y(ups[d])))
-
+    for d in FAR_FIRST:
+        start(remote(sums.at[1], sums_in.at[7 + d], sz_s.at[d], sz_r.at[d], at_z(zup[d])))
+    for k in Z_ORDER[4:]:
+        z_wait(d_blk, dz_s, dz_r, k)
+        y_send(d_blk, dy_s, dy_r, k)
+    for k in order:
+        for way in (0, 1):
+            y_wait(d_blk, dy_s, dy_r, way, k)
+        w_send(d_blk, dw_s, dw_r, k)
+    for d in Z_ORDER:
+        remote(sums.at[1], sums_in.at[7 + d], sz_s.at[d], sz_r.at[d], at_z(zup[d])).wait_recv()
+        total = total + sums_in[7 + d]
+    sums[2] = total
+    for d in (2, 1, 3):
+        start(remote(sums.at[2], sums_in.at[14 + d], sy_s.at[d], sy_r.at[d], at_y(ups[d])))
     for k in order:
         w_wait(d_blk, dw_s, dw_r, k)
     every = drc[...].astype(F32).reshape(32, 16, 256)
     pq[...] = dot(factor(0, 16), every[:, 0:8].reshape(256, 256).astype(BF16))
     po[...] = dot(factor(16, 32), every[:, 8:16].reshape(256, 256).astype(BF16))
     for d in (1, 2, 3):
-        remote(sums.at[1], sums_in.at[7 + d], sy_s.at[d], sy_r.at[d], at_y(ups[d])).wait_recv()
-        total = total + sums_in[7 + d]
+        remote(sums.at[2], sums_in.at[14 + d], sy_s.at[d], sy_r.at[d], at_y(ups[d])).wait_recv()
+        total = total + sums_in[14 + d]
     count = 256.0 * 8 * qcols
     scale_q = lax.rsqrt(total[0:1, 0:1] / count + 0.25)
     scale_o = lax.rsqrt(total[4:5, 0:1] / (256.0 * 8 * 256) + 0.25)
@@ -308,23 +302,25 @@
     so_v[...] = own_o
     nq_v[...] = qw_v[...] - 0.02 * own_q
     no_v[...] = ow_v[...] - 0.02 * own_o
-    put(sq_v, step_q)
-    put(so_v, step_o)
-    put(nq_v, new_q)
-    put(no_v, new_o)
     for i in (0, 1):
         dst = wei.at[pl.ds(4 * i, 4), ups[2]]
         remote(dst, dst, ww_s.at[i], ww_r.at[i], at_y(ups[1])).wait_recv()
     weights = wei[...].reshape(32, 48, 256).astype(F32)
     weights_q = weights[:, 0:16].reshape(512, 256)
     weights_o = weights[:, 16:48].reshape(1024, 256)
-    cq[...] = (weights_q - 0.02 * (pq[...] * scale_q))[:, 0:qcols].astype(BF16)
-    put(cq, copy_q)
+    cq[...] = (weights_q - 0.02 * (pq[...] * scale_q)).T[0:qcols, :].astype(BF16)
     co[...] = (weights_o - 0.02 * (po[...] * scale_o)).astype(BF16)
-    put(co, copy_o)
     for copy in started:
         copy.wait_send()
-    for copy in outs:
+
+
+def write_out(*refs):
+    n = len(refs) // 2
+    sem = refs[-1]
+    copies = [pltpu.make_async_copy(refs[i], refs[n + i], sem.at[i]) for i in range(n)]
+    for copy in copies:
+        copy.start()
+    for copy in copies:
         copy.wait()
 
 
@@ -343,14 +339,15 @@
         any_ = pl.BlockSpec(memory_space=pl.ANY)
         outs = (
             like(qw), like(ow), like(qw), like(ow),
-            jax.ShapeDtypeStruct((512, qcols), BF16), jax.ShapeDtypeStruct((1024, 256), BF16),
+            jax.ShapeDtypeStruct((qcols, 512), BF16), jax.ShapeDtypeStruct((1024, 256), BF16),
             like(qm), like(qs), like(om), like(os_),
         )
-        return pl.pallas_call(
+        qcot = qcot.T
+        held = pl.pallas_call(
             functools.partial(kernel, inv_root),
-            out_shape=outs,
+            out_shape=[pltpu.VMEM(a.shape, a.dtype) for a in outs],
             in_specs=[any_] * 12,
-            out_specs=[any_] * 10,
+            out_specs=[pl.BlockSpec(memory_space=pltpu.VMEM)] * 10,
             scratch_shapes=[
                 vm(lat), vm(qcot), vm(att), vm(mix), vm(qw), vm(ow), vm(qm), vm(qs), vm(om), vm(os_),
                 pltpu.VMEM((qcols, 512), F32), pltpu.VMEM((256, 1024), F32),
@@ -358,21 +355,27 @@
                 pltpu.VMEM((NY, NZ, 16, 256), BF16), pltpu.VMEM((NY, NZ, 16, 256), BF16),
                 pltpu.VMEM((NZ, 16, 256), BF16), pltpu.VMEM((NZ, 16, 256), BF16),
                 pltpu.VMEM((NZ, NY, 16, 256), BF16),
-                pltpu.VMEM((2, 8, 128), F32), pltpu.VMEM((11, 8, 128), F32),
+                pltpu.VMEM((3, 8, 128), F32), pltpu.VMEM((18, 8, 128), F32),
                 pltpu.VMEM((512, 256), F32), pltpu.VMEM((1024, 256), F32),
-                pltpu.VMEM((512, qcols), BF16), pltpu.VMEM((1024, 256), BF16),
-                vm(qw), vm(ow), vm(qw), vm(ow), vm(qm), vm(qs), vm(om), vm(os_),
-                dma((CHUNKS, 4)), dma((8,)), dma((10,)),
+                dma((CHUNKS, 4)), dma((8,)),
                 dma((8,)), dma((8,)), dma((2, 8)), dma((2, 8)), dma((8,)), dma((8,)), dma((4,)), dma((4,)),
                 dma((8,)), dma((8,)), dma((2,)), dma((2,)), dma((2,)), dma((2,)),
                 dma((4,)), dma((4,)), dma((8,)), dma((8,)),
                 dma((8,)), dma((8,)), dma((2, 8)), dma((2, 8)), dma((8,)), dma((8,)),
-                dma((8,)), dma((8,)), dma((4,)), dma((4,)),
+                dma((8,)), dma((8,)), dma((8,)), dma((8,)), dma((4,)), dma((4,)),
             ],
             compiler_params=pltpu.CompilerParams(
                 collective_id=0, has_side_effects=True, vmem_limit_bytes=56 * 1024 * 1024
             ),
         )(lat, qcot, att, mix, qw, ow, qf, of, qm, qs, om, os_)
+        results = pl.pallas_call(
+            write_out,
+            out_shape=outs,
+            in_specs=[pl.BlockSpec(memory_space=pltpu.VMEM)] * 10,
+            out_specs=[any_] * 10,
+            scratch_shapes=[dma((10,))],
+        )(*[pltpu.with_memory_space_constraint(a, pltpu.VMEM) for a in held])
+        return (*results[:4], results[4].T, *results[5:])
 
     rows, both, whole = P("fs", None), P("fs", "tp"), P(None, "tp")
     return jax.shard_map(

time: 66.8 us -> 49 us (0.73)
  local copies, waits for them, and re-layouts: 14 us -> 0 us
  Pallas kernels: 51.7 us -> 48.2 us
    unnamed x18 -> x0, local copies, waits for them, and re-layouts: 12.2 us -> none
    pallas_call x1 -> x2, Pallas kernels: 51.7 us -> 48.2 us  [the longest x1 47.2 us: on_device(): pl.pallas_call(functools.partial(kernel, inv_root), out_shape=[pltpu.VMEM...]
    pallas_call x1 -> x0, local copies, waits for them, and re-layouts: 1.78 us -> none  [on_device(): pl.pallas_call(functools.partial(kernel, inv_root), out_shape=outs, in_sp...]
where the time goes in v2:
time: 49 us; the launch traced here: 48.9 us
  Pallas kernels  48.2 us (98%)
  between operations  0.66 us (1%)
    pallas_call x1, Pallas kernels, on_device(): pl.pallas_call(functools.partial(kernel, inv_root), out_shape=[pltpu.VMEM...  47.2 us
    pallas_call x1, Pallas kernels, on_device(): pl.pallas_call(write_out, out_shape=outs, in_specs=[pl.BlockSpec(memory_s...  0.99 us

profile of v2, /device:TPU:1, one launch (start us, length us, event | category | flops | bytes accessed | tf_op | source)
XLA Modules:
  0.0 48.9 jit_solution(17380785698999724524)
XLA Ops:
  0.6 47.2 %shard_map.195 = (f32[16,192]{1,0:T(8,128)S(1)}, f32[32,256]{1,0:T(8,128)S(1)}, f32[16,192]{1,0:T(8,128)S(1)}, f32[32,256]{1,0:T(8,128)S(1)}, bf16[192,512]{1,0:...) custom-call(bf16[3072,512]{1,0:T(8,128)(2,1)} %lat.1, ...), custom_call_target="tpu_custom_call" | custom-call | tf_op jit(solution)/shard_map/pallas_call | solution.py:346
  47.9 1.0 %shard_map.196 = (f32[16,192]{1,0:T(8,128)}, f32[32,256]{1,0:T(8,128)}, f32[16,192]{1,0:T(8,128)}, f32[32,256]{1,0:T(8,128)}, bf16[192,512]{1,0:T(8,128)(2,1)}, ...) custom-call(f32[16,192]{1,0:T(8,128)S(1)} %get-tuple-element.30.refs, ...), custom_call_target="tpu_custom_call" | custom-call | tf_op jit(solution)/shard_map/pallas_call | solution.py:371

commit v3 on v2

v3 whole, which is shorter than its diff:
```python
import functools
import math

import jax
import jax.numpy as jnp
from jax import lax
from jax.experimental import pallas as pl
from jax.experimental.pallas import tpu as pltpu
from jax.sharding import PartitionSpec as P

MESH = pl.DeviceIdType.MESH
F32 = jnp.float32
BF16 = jnp.bfloat16
NZ, NY = 8, 4
CHUNKS = 6
Z_ORDER = (1, 7, 2, 6, 3, 5, 4)
FAR_FIRST = (4, 3, 5, 2, 6, 1, 7)
SIDE = [(d, e) for d in range(NY) for e in range(8) if d or e]


def by_tokens(left, right):
    return lax.dot_general(left, right, (((0,), (0,)), ((), ())), preferred_element_type=F32)


def dot(left, right):
    return jnp.dot(left, right, preferred_element_type=F32)


def kernel(
    inv_root,
    lat, qcot, att, mix, qw, ow, qf, of, qm, qs, om, os_,
    sq_v, so_v, nq_v, no_v, cq, co, mq_v, sqq_v, mo_v, soo_v,
    lat_v, qcot_v, att_v, mix_v, qw_v, ow_v, qm_v, qs_v, om_v, os_v,
    gq, go, fac, wei, part, part_in, mid, mid_in, drc, sums, sums_in,
    pq, po,
    chunk_sem, small_sem,
    fz_s, fz_r, fy_s, fy_r, fd_s, fd_r,
    wz_s, wz_r, wy_s, wy_r, wb_s, wb_r, wc_s, wc_r,
    py_s, py_r, pz_s, pz_r,
    dz_s, dz_r, dy_s, dy_r,
    sz_s, sz_r,
):
    fs, tp = lax.axis_index("fs"), lax.axis_index("tp")
    y, z = lax.rem(fs, NY), fs // NY
    core = lax.rem(tp, 2)
    other = 1 - core
    partner = (fs, tp + 1 - 2 * core)
    ups = [lax.rem(y + d, NY) for d in range(NY)]
    downs = [lax.rem(y + NY - d, NY) for d in range(NY)]
    zup = [lax.rem(z + d, NZ) for d in range(NZ)]
    zdn = [lax.rem(z + NZ - d, NZ) for d in range(NZ)]

    def at_y(row):
        return (z * NY + row, tp)

    def at_z(level):
        return (level * NY + y, tp)

    def side(d, e):
        return (z * NY + ups[d], lax.rem(tp + e, 8))

    def remote(src, dst, send, recv, to):
        return pltpu.make_async_remote_copy(
            src_ref=src, dst_ref=dst, send_sem=send, recv_sem=recv, device_id=to, device_id_type=MESH
        )

    half = pl.ds(pl.multiple_of(core * 128, 128), 128)
    own = fac.at[core, z, y]
    small = []
    for i, (src, dst) in enumerate((
        (qf.at[:, half], own.at[pl.ds(0, 16)]),
        (of.at[:, half], own.at[pl.ds(16, 32)]),
        (qw, qw_v), (ow, ow_v), (qm, qm_v), (qs, qs_v), (om, om_v), (os_, os_v),
    )):
        small.append(pltpu.make_async_copy(src, dst, small_sem.at[i]))
        small[-1].start()

    barrier = pltpu.get_barrier_semaphore()
    for to in [at_z(zup[d]) for d in range(1, NZ)] + [side(d, e) for d, e in SIDE]:
        pl.semaphore_signal(barrier, inc=1, device_id=to, device_id_type=MESH)

    tokens = lat.shape[0]
    rows = tokens // CHUNKS
    pairs = ((lat, lat_v), (mix, mix_v), (att, att_v))

    def chunk_copies(i):
        span = pl.ds(pl.multiple_of(i * rows, rows), rows)
        copies = [
            pltpu.make_async_copy(src.at[span], dst.at[span], chunk_sem.at[i, j])
            for j, (src, dst) in enumerate(pairs)
        ]
        copies.append(pltpu.make_async_copy(qcot.at[:, span], qcot_v.at[:, span], chunk_sem.at[i, 3]))
        return copies

    def add_chunk(i):
        for copy in chunk_copies(i):
            copy.wait()
        span = pl.ds(pl.multiple_of(i * rows, rows), rows)
        gq[...] += dot(qcot_v[:, span], lat_v[span, :])
        go[...] += by_tokens(mix_v[span, :], att_v[span, :])

    def add_chunks(a, b):
        @pl.loop(a, b)
        def _(i):
            add_chunk(i)

    for copy in small[:4]:
        copy.wait()
    for i in range(CHUNKS):
        for copy in chunk_copies(i):
            copy.start()
    qcols = qw_v.shape[1]
    wei[0, z, y, 0:16] = qw_v[:, 0:128].astype(BF16)
    wei[1, z, y, 0:16, 0:qcols - 128] = qw_v[:, 128:qcols].astype(BF16)
    for i in (0, 1):
        wei[i, z, y, 16:48] = ow_v[:, 128 * i:128 * i + 128].astype(BF16)

    pl.semaphore_wait(barrier, 38)

    def f_blk(level, row):
        return fac.at[core, level, row]

    def w_blk(level, row):
        return wei.at[0, level, row]

    def d_blk(level, row):
        return drc.at[level, row]

    started = []

    def start(copy):
        copy.start()
        started.append(copy)

    def z_send(blk, s, r):
        for k in FAR_FIRST:
            start(remote(blk(z, y), blk(z, y), s.at[k], r.at[k], at_z(zup[k])))

    def z_wait(blk, s, r, k):
        remote(blk(zdn[k], y), blk(zdn[k], y), s.at[k], r.at[k], at_z(zup[k])).wait_recv()

    def y_send(blk, s, r, k):
        for d in (2, 1, 3):
            start(remote(blk(zdn[k], y), blk(zdn[k], y), s.at[d, k], r.at[d, k], at_y(ups[d])))

    def y_wait(blk, s, r, d, k):
        dst = blk(zdn[k], downs[d])
        remote(dst, dst, s.at[d, k], r.at[d, k], at_y(ups[d])).wait_recv()

    def swap_send(d, k):
        src = f_blk(zdn[k], downs[d])
        start(remote(src, src, fd_s.at[d, k], fd_r.at[d, k], partner))

    def swap_wait(d, k):
        dst = fac.at[other, zdn[k], downs[d]]
        remote(dst, dst, fd_s.at[d, k], fd_r.at[d, k], partner).wait_recv()

    z_send(f_blk, fz_s, fz_r)
    y_send(f_blk, fy_s, fy_r, 0)
    swap_send(0, 0)
    for d in (2, 1, 3):
        src = wei.at[1, z, y]
        start(remote(src, src, wb_s.at[d], wb_r.at[d], at_y(ups[d])))
    gq[...] = jnp.zeros_like(gq)
    go[...] = jnp.zeros_like(go)
    add_chunks(0, 4)

    def pass_on(k):
        z_wait(f_blk, fz_s, fz_r, k)
        y_send(f_blk, fy_s, fy_r, k)
        swap_send(0, k)

    for k in Z_ORDER[:2]:
        pass_on(k)
    add_chunks(4, CHUNKS)
    for k in Z_ORDER[2:]:
        pass_on(k)
    z_send(w_blk, wz_s, wz_r)
    for d in (1, 3, 2):
        dst = wei.at[1, z, downs[d]]
        remote(dst, dst, wb_s.at[d], wb_r.at[d], at_y(ups[d])).wait_recv()
    for k in FAR_FIRST:
        src = wei.at[1, z]
        start(remote(src, src, wc_s.at[k], wc_r.at[k], at_z(zup[k])))
    order = (0,) + Z_ORDER
    for k in order:
        for d in (1, 3, 2):
            y_wait(f_blk, fy_s, fy_r, d, k)
            swap_send(d, k)
    for k in order:
        for d in range(NY):
            swap_wait(d, k)

    def factor(first, count):
        return jnp.concatenate(
            [fac[c, :, :, first:first + count, :].reshape(32 * count, 128) for c in (0, 1)], axis=1
        )

    low_q = dot(gq[...].astype(BF16), factor(0, 16)) * inv_root
    low_q = jnp.concatenate([low_q, jnp.zeros((256 - qcols, 256), F32)], axis=0).T
    low_o = (dot(go[...].astype(BF16), factor(16, 32)) * inv_root).T
    low_q, low_o = low_q.reshape(NZ, NY, 8, 256), low_o.reshape(NZ, NY, 8, 256)
    turn = [lax.rem(lev + 2 * NZ - 3 - z, NZ) for lev in range(NZ)]
    for lev in range(NZ):
        for row in range(NY):
            part[row, turn[lev]] = jnp.concatenate([low_q[lev, row], low_o[lev, row]], axis=0).astype(BF16)

    pieces = (pl.ds(0, 3), pl.ds(3, 5))
    for i, piece in enumerate(pieces):
        for d in (2, 1, 3):
            src = part.at[ups[d], piece]
            start(remote(src, part_in.at[d, piece], py_s.at[i, d], py_r.at[i, d], at_y(ups[d])))
    for i, piece in enumerate(pieces):
        total = part[y, piece].astype(F32)
        for d in (1, 3, 2):
            src = part.at[y, piece]
            remote(src, part_in.at[d, piece], py_s.at[i, d], py_r.at[i, d], at_y(ups[d])).wait_recv()
            total = total + part_in[d, piece].astype(F32)
        mid[piece] = total.astype(BF16)
        for k in (4, 3, 5) if i == 0 else (2, 6, 1, 7):
            src = mid.at[(k + NZ - 3) % NZ]
            start(remote(src, mid_in.at[k], pz_s.at[k], pz_r.at[k], at_z(zup[k])))
    for k in Z_ORDER:
        z_wait(w_blk, wz_s, wz_r, k)
    for d in (2, 1, 3):
        src = wei.at[0, :, y]
        start(remote(src, src, wy_s.at[d], wy_r.at[d], at_y(ups[d])))
    low = mid[5].astype(F32)
    for k in Z_ORDER:
        remote(mid.at[5], mid_in.at[k], pz_s.at[k], pz_r.at[k], at_z(zup[k])).wait_recv()
        low = low + mid_in[k].astype(F32)

    def moments(mean, square, low):
        mean_new = 0.8 * mean + 0.2 * low
        square_new = 0.9 * square + 0.1 * low * low
        return (mean_new, square_new, mean_new / jnp.sqrt(square_new))

    for copy in small[4:]:
        copy.wait()
    mq_v[...], sqq_v[...], dir_q = moments(qm_v[...], qs_v[...], low[0:8, 0:qcols])
    mo_v[...], soo_v[...], dir_o = moments(om_v[...], os_v[...], low[8:16, :])
    dir_q = jnp.concatenate([dir_q, jnp.zeros((8, 256 - qcols), F32)], axis=1)
    drc[z, y] = jnp.concatenate([dir_q, dir_o], axis=0).astype(BF16)
    sent = len(started) - 3
    z_send(d_blk, dz_s, dz_r)
    y_send(d_blk, dy_s, dy_r, 0)

    def squares(rows):
        both = rows.astype(F32)
        return both * both

    for copy in started[:sent]:
        copy.wait_send()
    square = squares(drc[z, y])
    for k in Z_ORDER[:4]:
        z_wait(d_blk, dz_s, dz_r, k)
        y_send(d_blk, dy_s, dy_r, k)
        square = square + squares(drc[zdn[k], y])
    for k in Z_ORDER[4:]:
        z_wait(d_blk, dz_s, dz_r, k)
        y_send(d_blk, dy_s, dy_r, k)
    for k in Z_ORDER[4:]:
        square = square + squares(drc[zdn[k], y])
    sum_q = jnp.sum(square[0:8], axis=(0, 1), keepdims=True)
    sum_o = jnp.sum(square[8:16], axis=(0, 1), keepdims=True)
    sums[0] = jnp.concatenate([jnp.broadcast_to(sum_q, (1, 64)), jnp.broadcast_to(sum_o, (1, 64))], axis=1)
    for i, (d, e) in enumerate(SIDE):
        start(remote(sums.at[0], sums_in.at[i], sz_s.at[i], sz_r.at[i], side(d, e)))
    for k in order:
        for d in (1, 3, 2):
            y_wait(d_blk, dy_s, dy_r, d, k)
    every = drc[...].astype(F32).reshape(32, 16, 256)
    pq[...] = dot(factor(0, 16), every[:, 0:8].reshape(256, 256).astype(BF16))
    po[...] = dot(factor(16, 32), every[:, 8:16].reshape(256, 256).astype(BF16))
    total = sums[0]
    for i in range(31):
        remote(sums.at[0], sums_in.at[i], sz_s.at[i], sz_r.at[i], partner).wait_recv()
        total = total + sums_in[i]
    count = 256.0 * 8 * qcols
    scale_q = lax.rsqrt(total[0:1, 0:1] / count + 0.25)
    scale_o = lax.rsqrt(total[0:1, 64:65] / (256.0 * 8 * 256) + 0.25)

    own_q = pq[pl.ds(pl.multiple_of(fs * 16, 16), 16), :][:, 0:qcols] * scale_q
    own_o = po[pl.ds(pl.multiple_of(fs * 32, 32), 32), :] * scale_o
    sq_v[...] = own_q
    so_v[...] = own_o
    nq_v[...] = qw_v[...] - 0.02 * own_q
    no_v[...] = ow_v[...] - 0.02 * own_o
    for d in (1, 3, 2):
        dst = wei.at[0, :, downs[d]]
        remote(dst, dst, wy_s.at[d], wy_r.at[d], at_y(ups[d])).wait_recv()
    for k in Z_ORDER:
        dst = wei.at[1, zdn[k]]
        remote(dst, dst, wc_s.at[k], wc_r.at[k], at_z(zup[k])).wait_recv()
    weights = jnp.concatenate([wei[0].reshape(32, 48, 128), wei[1].reshape(32, 48, 128)], axis=2).astype(F32)
    weights_q = weights[:, 0:16].reshape(512, 256)
    weights_o = weights[:, 16:48].reshape(1024, 256)
    cq[...] = (weights_q - 0.02 * (pq[...] * scale_q)).T[0:qcols, :].astype(BF16)
    co[...] = (weights_o - 0.02 * (po[...] * scale_o)).astype(BF16)
    for copy in started[sent:]:
        copy.wait_send()


def write_out(*refs):
    n = len(refs) // 2
    sem = refs[-1]
    copies = [pltpu.make_async_copy(refs[i], refs[n + i], sem.at[i]) for i in range(n)]
    for copy in copies:
        copy.start()
    for copy in copies:
        copy.wait()


def solution(mesh):
    def on_device(lat, qcot, att, mix, qw, ow, qf, of, qm, qs, om, os_):
        tokens, qcols = lat.shape[0], qw.shape[1]
        inv_root = 1.0 / math.sqrt(tokens * lax.axis_size("fs"))

        def like(a):
            return jax.ShapeDtypeStruct(a.shape, a.dtype)

        def vm(a):
            return pltpu.VMEM(a.shape, a.dtype)

        dma = pltpu.SemaphoreType.DMA
        any_ = pl.BlockSpec(memory_space=pl.ANY)
        outs = (
            like(qw), like(ow), like(qw), like(ow),
            jax.ShapeDtypeStruct((qcols, 512), BF16), jax.ShapeDtypeStruct((1024, 256), BF16),
            like(qm), like(qs), like(om), like(os_),
        )
        qcot = qcot.T
        held = pl.pallas_call(
            functools.partial(kernel, inv_root),
            out_shape=[pltpu.VMEM(a.shape, a.dtype) for a in outs],
            in_specs=[any_] * 12,
            out_specs=[pl.BlockSpec(memory_space=pltpu.VMEM)] * 10,
            scratch_shapes=[
                vm(lat), vm(qcot), vm(att), vm(mix), vm(qw), vm(ow), vm(qm), vm(qs), vm(om), vm(os_),
                pltpu.VMEM((qcols, 512), F32), pltpu.VMEM((256, 1024), F32),
                pltpu.VMEM((2, NZ, NY, 48, 128), BF16), pltpu.VMEM((2, NZ, NY, 48, 128), BF16),
                pltpu.VMEM((NY, NZ, 16, 256), BF16), pltpu.VMEM((NY, NZ, 16, 256), BF16),
                pltpu.VMEM((NZ, 16, 256), BF16), pltpu.VMEM((NZ, 16, 256), BF16),
                pltpu.VMEM((NZ, NY, 16, 256), BF16),
                pltpu.VMEM((1, 1, 128), F32), pltpu.VMEM((31, 1, 128), F32),
                pltpu.VMEM((512, 256), F32), pltpu.VMEM((1024, 256), F32),
                dma((CHUNKS, 4)), dma((8,)),
                dma((8,)), dma((8,)), dma((4, 8)), dma((4, 8)), dma((4, 8)), dma((4, 8)),
                dma((8,)), dma((8,)), dma((4,)), dma((4,)), dma((4,)), dma((4,)), dma((8,)), dma((8,)),
                dma((2, 4)), dma((2, 4)), dma((8,)), dma((8,)),
                dma((8,)), dma((8,)), dma((4, 8)), dma((4, 8)),
                dma((31,)), dma((31,)),
            ],
            compiler_params=pltpu.CompilerParams(
                collective_id=0, has_side_effects=True, vmem_limit_bytes=56 * 1024 * 1024
            ),
        )(lat, qcot, att, mix, qw, ow, qf, of, qm, qs, om, os_)
        results = pl.pallas_call(
            write_out,
            out_shape=outs,
            in_specs=[pl.BlockSpec(memory_space=pltpu.VMEM)] * 10,
            out_specs=[any_] * 10,
            scratch_shapes=[dma((10,))],
        )(*[pltpu.with_memory_space_constraint(a, pltpu.VMEM) for a in held])
        return (*results[:4], results[4].T, *results[5:])

    rows, both, whole = P("fs", None), P("fs", "tp"), P(None, "tp")
    return jax.shard_map(
        on_device,
        mesh=mesh,
        in_specs=(rows, both, rows, both, both, both, rows, rows, both, both, both, both),
        out_specs=(both, both, both, both, whole, whole, both, both, both, both),
        check_vma=False,
    )
```

time: 49 us -> 45.4 us (0.927)
  Pallas kernels: 48.2 us -> 44.6 us
    pallas_call x1, Pallas kernels: 47.2 us -> 43.6 us  [on_device(): pl.pallas_call(functools.partial(kernel, inv_root), out_shape=[pltpu.VMEM...]
where the time goes in v3:
time: 45.4 us; the launch traced here: 45.3 us
  Pallas kernels  44.6 us (98%)
  between operations  0.66 us (1%)
    pallas_call x1, Pallas kernels, on_device(): pl.pallas_call(functools.partial(kernel, inv_root), out_shape=[pltpu.VMEM...  43.6 us
    pallas_call x1, Pallas kernels, on_device(): pl.pallas_call(write_out, out_shape=outs, in_specs=[pl.BlockSpec(memory_s...  0.99 us

profile of v3, /device:TPU:1, one launch (start us, length us, event | category | flops | bytes accessed | tf_op | source)
XLA Modules:
  0.0 45.3 jit_solution(6736028547348000084)
XLA Ops:
  0.6 43.6 %shard_map.195 = (f32[16,192]{1,0:T(8,128)S(1)}, f32[32,256]{1,0:T(8,128)S(1)}, f32[16,192]{1,0:T(8,128)S(1)}, f32[32,256]{1,0:T(8,128)S(1)}, bf16[192,512]{1,0:...) custom-call(bf16[3072,512]{1,0:T(8,128)(2,1)} %lat.1, ...), custom_call_target="tpu_custom_call" | custom-call | tf_op jit(solution)/shard_map/pallas_call | solution.py:333
  44.3 1.0 %shard_map.196 = (f32[16,192]{1,0:T(8,128)}, f32[32,256]{1,0:T(8,128)}, f32[16,192]{1,0:T(8,128)}, f32[32,256]{1,0:T(8,128)}, bf16[192,512]{1,0:T(8,128)(2,1)}, ...) custom-call(f32[16,192]{1,0:T(8,128)S(1)} %get-tuple-element.30.refs, ...), custom_call_target="tpu_custom_call" | custom-call | tf_op jit(solution)/shard_map/pallas_call | solution.py:358

commit v4 on v3

--- a/solution.py
+++ b/solution.py
@@ -38,7 +38,7 @@
     wz_s, wz_r, wy_s, wy_r, wb_s, wb_r, wc_s, wc_r,
     py_s, py_r, pz_s, pz_r,
     dz_s, dz_r, dy_s, dy_r,
-    sz_s, sz_r,
+    sx_s, sx_r, sz_s, sz_r,
 ):
     fs, tp = lax.axis_index("fs"), lax.axis_index("tp")
     y, z = lax.rem(fs, NY), fs // NY
@@ -163,18 +163,22 @@
         start(remote(src, src, wb_s.at[d], wb_r.at[d], at_y(ups[d])))
     gq[...] = jnp.zeros_like(gq)
     go[...] = jnp.zeros_like(go)
-    add_chunks(0, 4)
 
     def pass_on(k):
         z_wait(f_blk, fz_s, fz_r, k)
         y_send(f_blk, fy_s, fy_r, k)
         swap_send(0, k)
 
+    add_chunks(0, 3)
     for k in Z_ORDER[:2]:
         pass_on(k)
-    add_chunks(4, CHUNKS)
-    for k in Z_ORDER[2:]:
+    add_chunks(3, 4)
+    for k in Z_ORDER[2:4]:
         pass_on(k)
+    add_chunks(4, 5)
+    for k in Z_ORDER[4:]:
+        pass_on(k)
+    add_chunks(5, 6)
     z_send(w_blk, wz_s, wz_r)
     for d in (1, 3, 2):
         dst = wei.at[1, z, downs[d]]
@@ -245,37 +249,46 @@
     z_send(d_blk, dz_s, dz_r)
     y_send(d_blk, dy_s, dy_r, 0)
 
-    def squares(rows):
-        both = rows.astype(F32)
-        return both * both
-
+    sum_q = jnp.sum(dir_q * dir_q, axis=(0, 1), keepdims=True)
+    sum_o = jnp.sum(dir_o * dir_o, axis=(0, 1), keepdims=True)
+    sums[0] = jnp.concatenate([jnp.broadcast_to(sum_q, (1, 64)), jnp.broadcast_to(sum_o, (1, 64))], axis=1)
+    for i, (d, e) in enumerate(SIDE):
+        start(remote(sums.at[0], sums_in.at[i], sx_s.at[i], sx_r.at[i], side(d, e)))
     for copy in started[:sent]:
         copy.wait_send()
-    square = squares(drc[z, y])
     for k in Z_ORDER[:4]:
         z_wait(d_blk, dz_s, dz_r, k)
         y_send(d_blk, dy_s, dy_r, k)
-        square = square + squares(drc[zdn[k], y])
     for k in Z_ORDER[4:]:
         z_wait(d_blk, dz_s, dz_r, k)
         y_send(d_blk, dy_s, dy_r, k)
-    for k in Z_ORDER[4:]:
-        square = square + squares(drc[zdn[k], y])
-    sum_q = jnp.sum(square[0:8], axis=(0, 1), keepdims=True)
-    sum_o = jnp.sum(square[8:16], axis=(0, 1), keepdims=True)
-    sums[0] = jnp.concatenate([jnp.broadcast_to(sum_q, (1, 64)), jnp.broadcast_to(sum_o, (1, 64))], axis=1)
-    for i, (d, e) in enumerate(SIDE):
-        start(remote(sums.at[0], sums_in.at[i], sz_s.at[i], sz_r.at[i], side(d, e)))
+    total = sums[0]
+    for i in range(31):
+        remote(sums.at[0], sums_in.at[i], sx_s.at[i], sx_r.at[i], partner).wait_recv()
+        total = total + sums_in[i]
+    sums[1] = total
+
+    def sum_copies():
+        return [
+            remote(sums.at[1], sums_in.at[31 + k], sz_s.at[c, k], sz_r.at[k], (zup[k] * NY + y, tp - c))
+            for k in FAR_FIRST
+            for c in (1, 0)
+        ]
+
+    @pl.when(core == 1)
+    def _():
+        for copy in sum_copies():
+            copy.start()
+
     for k in order:
         for d in (1, 3, 2):
             y_wait(d_blk, dy_s, dy_r, d, k)
     every = drc[...].astype(F32).reshape(32, 16, 256)
     pq[...] = dot(factor(0, 16), every[:, 0:8].reshape(256, 256).astype(BF16))
     po[...] = dot(factor(16, 32), every[:, 8:16].reshape(256, 256).astype(BF16))
-    total = sums[0]
-    for i in range(31):
-        remote(sums.at[0], sums_in.at[i], sz_s.at[i], sz_r.at[i], partner).wait_recv()
-        total = total + sums_in[i]
+    for k in Z_ORDER:
+        remote(sums.at[1], sums_in.at[31 + k], sz_s.at[0, k], sz_r.at[k], at_z(zup[k])).wait_recv()
+        total = total + sums_in[31 + k]
     count = 256.0 * 8 * qcols
     scale_q = lax.rsqrt(total[0:1, 0:1] / count + 0.25)
     scale_o = lax.rsqrt(total[0:1, 64:65] / (256.0 * 8 * 256) + 0.25)
@@ -299,6 +312,11 @@
     co[...] = (weights_o - 0.02 * (po[...] * scale_o)).astype(BF16)
     for copy in started[sent:]:
         copy.wait_send()
+
+    @pl.when(core == 1)
+    def _():
+        for copy in sum_copies():
+            copy.wait_send()
 
 
 def write_out(*refs):
@@ -342,14 +360,14 @@
                 pltpu.VMEM((NY, NZ, 16, 256), BF16), pltpu.VMEM((NY, NZ, 16, 256), BF16),
                 pltpu.VMEM((NZ, 16, 256), BF16), pltpu.VMEM((NZ, 16, 256), BF16),
                 pltpu.VMEM((NZ, NY, 16, 256), BF16),
-                pltpu.VMEM((1, 1, 128), F32), pltpu.VMEM((31, 1, 128), F32),
+                pltpu.VMEM((2, 1, 128), F32), pltpu.VMEM((39, 1, 128), F32),
                 pltpu.VMEM((512, 256), F32), pltpu.VMEM((1024, 256), F32),
                 dma((CHUNKS, 4)), dma((8,)),
                 dma((8,)), dma((8,)), dma((4, 8)), dma((4, 8)), dma((4, 8)), dma((4, 8)),
                 dma((8,)), dma((8,)), dma((4,)), dma((4,)), dma((4,)), dma((4,)), dma((8,)), dma((8,)),
                 dma((2, 4)), dma((2, 4)), dma((8,)), dma((8,)),
                 dma((8,)), dma((8,)), dma((4, 8)), dma((4, 8)),
-                dma((31,)), dma((31,)),
+                dma((31,)), dma((31,)), dma((2, 8)), dma((8,)),
             ],
             compiler_params=pltpu.CompilerParams(
                 collective_id=0, has_side_effects=True, vmem_limit_bytes=56 * 1024 * 1024

time: 45.4 us -> 44.3 us (0.976)
  Pallas kernels: 44.6 us -> 43.5 us
    pallas_call x1, Pallas kernels: 43.6 us -> 42.5 us  [on_device(): pl.pallas_call(functools.partial(kernel, inv_root), out_shape=[pltpu.VMEM...]
where the time goes in v4:
time: 44.3 us; the launch traced here: 44.2 us
  Pallas kernels  43.5 us (98%)
  between operations  0.66 us (1%)
    pallas_call x1, Pallas kernels, on_device(): pl.pallas_call(functools.partial(kernel, inv_root), out_shape=[pltpu.VMEM...  42.5 us
    pallas_call x1, Pallas kernels, on_device(): pl.pallas_call(write_out, out_shape=outs, in_specs=[pl.BlockSpec(memory_s...  0.99 us

profile of v4, /device:TPU:1, one launch (start us, length us, event | category | flops | bytes accessed | tf_op | source)
XLA Modules:
  0.0 44.2 jit_solution(17156930963586402474)
XLA Ops:
  0.6 42.5 %shard_map.195 = (f32[16,192]{1,0:T(8,128)S(1)}, f32[32,256]{1,0:T(8,128)S(1)}, f32[16,192]{1,0:T(8,128)S(1)}, f32[32,256]{1,0:T(8,128)S(1)}, bf16[192,512]{1,0:...) custom-call(bf16[3072,512]{1,0:T(8,128)(2,1)} %lat.1, ...), custom_call_target="tpu_custom_call" | custom-call | tf_op jit(solution)/shard_map/pallas_call | solution.py:351
  43.2 1.0 %shard_map.196 = (f32[16,192]{1,0:T(8,128)}, f32[32,256]{1,0:T(8,128)}, f32[16,192]{1,0:T(8,128)}, f32[32,256]{1,0:T(8,128)}, bf16[192,512]{1,0:T(8,128)(2,1)}, ...) custom-call(f32[16,192]{1,0:T(8,128)S(1)} %get-tuple-element.30.refs, ...), custom_call_target="tpu_custom_call" | custom-call | tf_op jit(solution)/shard_map/pallas_call | solution.py:376

commit v5 on v4

--- a/solution.py
+++ b/solution.py
@@ -15,6 +15,8 @@
 CHUNKS = 6
 Z_ORDER = (1, 7, 2, 6, 3, 5, 4)
 FAR_FIRST = (4, 3, 5, 2, 6, 1, 7)
+BY_DISTANCE = (4, 3, 5, 2, 6, 1, 7, 0)
+PIECES = ((0, 1), (1, 2), (3, 2), (5, 3))
 SIDE = [(d, e) for d in range(NY) for e in range(8) if d or e]
 
 
@@ -38,7 +40,7 @@
     wz_s, wz_r, wy_s, wy_r, wb_s, wb_r, wc_s, wc_r,
     py_s, py_r, pz_s, pz_r,
     dz_s, dz_r, dy_s, dy_r,
-    sx_s, sx_r, sz_s, sz_r,
+    sx_s, sx_r, sz_s, sz_r, met,
 ):
     fs, tp = lax.axis_index("fs"), lax.axis_index("tp")
     y, z = lax.rem(fs, NY), fs // NY
@@ -75,8 +77,9 @@
         small.append(pltpu.make_async_copy(src, dst, small_sem.at[i]))
         small[-1].start()
 
+    across = [(fs, lax.rem(tp + e, 8)) for e in (4, 2, 6)]
     barrier = pltpu.get_barrier_semaphore()
-    for to in [at_z(zup[d]) for d in range(1, NZ)] + [side(d, e) for d, e in SIDE]:
+    for to in [at_z(zup[k]) for k in FAR_FIRST] + [at_y(ups[d]) for d in (2, 1, 3)] + [partner] + across:
         pl.semaphore_signal(barrier, inc=1, device_id=to, device_id_type=MESH)
 
     tokens = lat.shape[0]
@@ -115,7 +118,7 @@
     for i in (0, 1):
         wei[i, z, y, 16:48] = ow_v[:, 128 * i:128 * i + 128].astype(BF16)
 
-    pl.semaphore_wait(barrier, 38)
+    pl.semaphore_wait(barrier, 14)
 
     def f_blk(level, row):
         return fac.at[core, level, row]
@@ -126,47 +129,41 @@
     def d_blk(level, row):
         return drc.at[level, row]
 
-    started = []
-
     def start(copy):
         copy.start()
-        started.append(copy)
+
+    def arrived(ref, sem):
+        pltpu.make_async_copy(ref, ref, sem).wait()
+
+    sent = arrived
 
     def z_send(blk, s, r):
         for k in FAR_FIRST:
-            start(remote(blk(z, y), blk(z, y), s.at[k], r.at[k], at_z(zup[k])))
-
-    def z_wait(blk, s, r, k):
-        remote(blk(zdn[k], y), blk(zdn[k], y), s.at[k], r.at[k], at_z(zup[k])).wait_recv()
+            start(remote(blk(z, y), blk(z, y), s, r.at[k], at_z(zup[k])))
+
+    def z_wait(blk, r, k):
+        arrived(blk(zdn[k], y), r.at[k])
 
     def y_send(blk, s, r, k):
         for d in (2, 1, 3):
-            start(remote(blk(zdn[k], y), blk(zdn[k], y), s.at[d, k], r.at[d, k], at_y(ups[d])))
-
-    def y_wait(blk, s, r, d, k):
-        dst = blk(zdn[k], downs[d])
-        remote(dst, dst, s.at[d, k], r.at[d, k], at_y(ups[d])).wait_recv()
+            start(remote(blk(zdn[k], y), blk(zdn[k], y), s, r(k), at_y(ups[d])))
 
     def swap_send(d, k):
         src = f_blk(zdn[k], downs[d])
-        start(remote(src, src, fd_s.at[d, k], fd_r.at[d, k], partner))
-
-    def swap_wait(d, k):
-        dst = fac.at[other, zdn[k], downs[d]]
-        remote(dst, dst, fd_s.at[d, k], fd_r.at[d, k], partner).wait_recv()
+        start(remote(src, src, fd_s, fd_r, partner))
 
     z_send(f_blk, fz_s, fz_r)
-    y_send(f_blk, fy_s, fy_r, 0)
+    y_send(f_blk, fy_s, fy_r.at.__getitem__, 0)
     swap_send(0, 0)
     for d in (2, 1, 3):
         src = wei.at[1, z, y]
-        start(remote(src, src, wb_s.at[d], wb_r.at[d], at_y(ups[d])))
+        start(remote(src, src, wb_s, wb_r, at_y(ups[d])))
     gq[...] = jnp.zeros_like(gq)
     go[...] = jnp.zeros_like(go)
 
     def pass_on(k):
-        z_wait(f_blk, fz_s, fz_r, k)
-        y_send(f_blk, fy_s, fy_r, k)
+        z_wait(f_blk, fz_r, k)
+        y_send(f_blk, fy_s, fy_r.at.__getitem__, k)
         swap_send(0, k)
 
     add_chunks(0, 3)
@@ -179,22 +176,21 @@
     for k in Z_ORDER[4:]:
         pass_on(k)
     add_chunks(5, 6)
-    z_send(w_blk, wz_s, wz_r)
-    for d in (1, 3, 2):
-        dst = wei.at[1, z, downs[d]]
-        remote(dst, dst, wb_s.at[d], wb_r.at[d], at_y(ups[d])).wait_recv()
+    for k in FAR_FIRST:
+        start(remote(w_blk(z, y), w_blk(z, y), wz_s, wz_r, at_z(zup[k])))
+    arrived(wei.at[1, 0, pl.ds(0, 3)], wb_r)
     for k in FAR_FIRST:
         src = wei.at[1, z]
-        start(remote(src, src, wc_s.at[k], wc_r.at[k], at_z(zup[k])))
+        start(remote(src, src, wc_s, wc_r, at_z(zup[k])))
     order = (0,) + Z_ORDER
     for k in order:
+        arrived(fac.at[core, 0, pl.ds(0, 3)], fy_r.at[k])
         for d in (1, 3, 2):
-            y_wait(f_blk, fy_s, fy_r, d, k)
             swap_send(d, k)
-    for k in order:
-        for d in range(NY):
-            swap_wait(d, k)
-
+    arrived(fac.at[other], fd_r)
+
+    for to in across:
+        pl.semaphore_signal(met, inc=1, device_id=to, device_id_type=MESH)
     def factor(first, count):
         return jnp.concatenate(
             [fac[c, :, :, first:first + count, :].reshape(32 * count, 128) for c in (0, 1)], axis=1
@@ -204,34 +200,37 @@
     low_q = jnp.concatenate([low_q, jnp.zeros((256 - qcols, 256), F32)], axis=0).T
     low_o = (dot(go[...].astype(BF16), factor(16, 32)) * inv_root).T
     low_q, low_o = low_q.reshape(NZ, NY, 8, 256), low_o.reshape(NZ, NY, 8, 256)
-    turn = [lax.rem(lev + 2 * NZ - 3 - z, NZ) for lev in range(NZ)]
     for lev in range(NZ):
+        k = lax.rem(lev + NZ - z, NZ)
+        upper = k // 4
+        place = 2 * (k - 4) * (2 * upper - 1) - (1 - upper)
         for row in range(NY):
-            part[row, turn[lev]] = jnp.concatenate([low_q[lev, row], low_o[lev, row]], axis=0).astype(BF16)
-
-    pieces = (pl.ds(0, 3), pl.ds(3, 5))
-    for i, piece in enumerate(pieces):
+            part[row, place] = jnp.concatenate([low_q[lev, row], low_o[lev, row]], axis=0).astype(BF16)
+
+    for i, (first, count) in enumerate(PIECES):
+        piece = pl.ds(first, count)
         for d in (2, 1, 3):
             src = part.at[ups[d], piece]
-            start(remote(src, part_in.at[d, piece], py_s.at[i, d], py_r.at[i, d], at_y(ups[d])))
-    for i, piece in enumerate(pieces):
+            start(remote(src, part_in.at[d, piece], py_s, py_r.at[i], at_y(ups[d])))
+    for i, (first, count) in enumerate(PIECES):
+        piece = pl.ds(first, count)
         total = part[y, piece].astype(F32)
-        for d in (1, 3, 2):
-            src = part.at[y, piece]
-            remote(src, part_in.at[d, piece], py_s.at[i, d], py_r.at[i, d], at_y(ups[d])).wait_recv()
+        arrived(part_in.at[pl.ds(1, 3), piece], py_r.at[i])
+        for d in (3, 1, 2):
             total = total + part_in[d, piece].astype(F32)
         mid[piece] = total.astype(BF16)
-        for k in (4, 3, 5) if i == 0 else (2, 6, 1, 7):
-            src = mid.at[(k + NZ - 3) % NZ]
-            start(remote(src, mid_in.at[k], pz_s.at[k], pz_r.at[k], at_z(zup[k])))
-    for k in Z_ORDER:
-        z_wait(w_blk, wz_s, wz_r, k)
+        for j in range(first, first + count):
+            k = BY_DISTANCE[j]
+            if k:
+                start(remote(mid.at[j], mid_in.at[k], pz_s, pz_r, at_z(zup[k])))
+    pl.semaphore_wait(met, 3)
+    arrived(wei.at[0, pl.ds(0, 7), 0], wz_r)
     for d in (2, 1, 3):
         src = wei.at[0, :, y]
-        start(remote(src, src, wy_s.at[d], wy_r.at[d], at_y(ups[d])))
-    low = mid[5].astype(F32)
+        start(remote(src, src, wy_s, wy_r, at_y(ups[d])))
+    arrived(mid_in.at[pl.ds(1, 7)], pz_r)
+    low = mid[7].astype(F32)
     for k in Z_ORDER:
-        remote(mid.at[5], mid_in.at[k], pz_s.at[k], pz_r.at[k], at_z(zup[k])).wait_recv()
         low = low + mid_in[k].astype(F32)
 
     def moments(mean, square, low):
@@ -245,32 +244,34 @@
     mo_v[...], soo_v[...], dir_o = moments(om_v[...], os_v[...], low[8:16, :])
     dir_q = jnp.concatenate([dir_q, jnp.zeros((8, 256 - qcols), F32)], axis=1)
     drc[z, y] = jnp.concatenate([dir_q, dir_o], axis=0).astype(BF16)
-    sent = len(started) - 3
     z_send(d_blk, dz_s, dz_r)
-    y_send(d_blk, dy_s, dy_r, 0)
+    y_send(d_blk, dy_s, lambda k: dy_r, 0)
 
     sum_q = jnp.sum(dir_q * dir_q, axis=(0, 1), keepdims=True)
     sum_o = jnp.sum(dir_o * dir_o, axis=(0, 1), keepdims=True)
     sums[0] = jnp.concatenate([jnp.broadcast_to(sum_q, (1, 64)), jnp.broadcast_to(sum_o, (1, 64))], axis=1)
     for i, (d, e) in enumerate(SIDE):
-        start(remote(sums.at[0], sums_in.at[i], sx_s.at[i], sx_r.at[i], side(d, e)))
-    for copy in started[:sent]:
-        copy.wait_send()
+        start(remote(sums.at[0], sums_in.at[i], sx_s, sx_r, side(d, e)))
+    sent(fac.at[core, pl.ds(0, 7), 0], fz_s)
+    sent(fac.at[core, pl.ds(0, 6)], fy_s)
+    sent(fac.at[core], fd_s)
+    sent(wei.at[1, 0, pl.ds(0, 3)], wb_s)
+    sent(wei.at[0, pl.ds(0, 7), 0], wz_s)
+    sent(part.at[pl.ds(0, 3)], py_s)
+    sent(mid.at[pl.ds(0, 7)], pz_s)
     for k in Z_ORDER[:4]:
-        z_wait(d_blk, dz_s, dz_r, k)
-        y_send(d_blk, dy_s, dy_r, k)
+        z_wait(d_blk, dz_r, k)
+        y_send(d_blk, dy_s, lambda k: dy_r, k)
     for k in Z_ORDER[4:]:
-        z_wait(d_blk, dz_s, dz_r, k)
-        y_send(d_blk, dy_s, dy_r, k)
-    total = sums[0]
-    for i in range(31):
-        remote(sums.at[0], sums_in.at[i], sx_s.at[i], sx_r.at[i], partner).wait_recv()
-        total = total + sums_in[i]
+        z_wait(d_blk, dz_r, k)
+        y_send(d_blk, dy_s, lambda k: dy_r, k)
+    arrived(sums_in.at[pl.ds(0, 31)], sx_r)
+    total = sums[0] + jnp.sum(sums_in[0:31], axis=0)
     sums[1] = total
 
     def sum_copies():
         return [
-            remote(sums.at[1], sums_in.at[31 + k], sz_s.at[c, k], sz_r.at[k], (zup[k] * NY + y, tp - c))
+            remote(sums.at[1], sums_in.at[31 + k], sz_s, sz_r, (zup[k] * NY + y, tp - c))
             for k in FAR_FIRST
             for c in (1, 0)
         ]
@@ -280,15 +281,12 @@
         for copy in sum_copies():
             copy.start()
 
-    for k in order:
-        for d in (1, 3, 2):
-            y_wait(d_blk, dy_s, dy_r, d, k)
+    arrived(drc.at[pl.ds(0, 6)], dy_r)
     every = drc[...].astype(F32).reshape(32, 16, 256)
     pq[...] = dot(factor(0, 16), every[:, 0:8].reshape(256, 256).astype(BF16))
     po[...] = dot(factor(16, 32), every[:, 8:16].reshape(256, 256).astype(BF16))
-    for k in Z_ORDER:
-        remote(sums.at[1], sums_in.at[31 + k], sz_s.at[0, k], sz_r.at[k], at_z(zup[k])).wait_recv()
-        total = total + sums_in[31 + k]
+    arrived(sums_in.at[pl.ds(32, 7)], sz_r)
+    total = total + jnp.sum(sums_in[32:39], axis=0)
     count = 256.0 * 8 * qcols
     scale_q = lax.rsqrt(total[0:1, 0:1] / count + 0.25)
     scale_o = lax.rsqrt(total[0:1, 64:65] / (256.0 * 8 * 256) + 0.25)
@@ -299,24 +297,22 @@
     so_v[...] = own_o
     nq_v[...] = qw_v[...] - 0.02 * own_q
     no_v[...] = ow_v[...] - 0.02 * own_o
-    for d in (1, 3, 2):
-        dst = wei.at[0, :, downs[d]]
-        remote(dst, dst, wy_s.at[d], wy_r.at[d], at_y(ups[d])).wait_recv()
-    for k in Z_ORDER:
-        dst = wei.at[1, zdn[k]]
-        remote(dst, dst, wc_s.at[k], wc_r.at[k], at_z(zup[k])).wait_recv()
+    arrived(wei.at[0, :, pl.ds(0, 3)], wy_r)
+    arrived(wei.at[1, pl.ds(0, 7)], wc_r)
     weights = jnp.concatenate([wei[0].reshape(32, 48, 128), wei[1].reshape(32, 48, 128)], axis=2).astype(F32)
     weights_q = weights[:, 0:16].reshape(512, 256)
     weights_o = weights[:, 16:48].reshape(1024, 256)
     cq[...] = (weights_q - 0.02 * (pq[...] * scale_q)).T[0:qcols, :].astype(BF16)
     co[...] = (weights_o - 0.02 * (po[...] * scale_o)).astype(BF16)
-    for copy in started[sent:]:
-        copy.wait_send()
+    sent(wei.at[1, pl.ds(0, 7)], wc_s)
+    sent(wei.at[0, :, pl.ds(0, 3)], wy_s)
+    sent(drc.at[pl.ds(0, 7), 0], dz_s)
+    sent(drc.at[pl.ds(0, 6)], dy_s)
+    sent(sums_in.at[pl.ds(0, 31)], sx_s)
 
     @pl.when(core == 1)
     def _():
-        for copy in sum_copies():
-            copy.wait_send()
+        sent(sums_in.at[pl.ds(0, 14)], sz_s)
 
 
 def write_out(*refs):
@@ -363,11 +359,11 @@
                 pltpu.VMEM((2, 1, 128), F32), pltpu.VMEM((39, 1, 128), F32),
                 pltpu.VMEM((512, 256), F32), pltpu.VMEM((1024, 256), F32),
                 dma((CHUNKS, 4)), dma((8,)),
-                dma((8,)), dma((8,)), dma((4, 8)), dma((4, 8)), dma((4, 8)), dma((4, 8)),
-                dma((8,)), dma((8,)), dma((4,)), dma((4,)), dma((4,)), dma((4,)), dma((8,)), dma((8,)),
-                dma((2, 4)), dma((2, 4)), dma((8,)), dma((8,)),
-                dma((8,)), dma((8,)), dma((4, 8)), dma((4, 8)),
-                dma((31,)), dma((31,)), dma((2, 8)), dma((8,)),
+                dma, dma((8,)), dma, dma((8,)), dma, dma,
+                dma, dma, dma, dma, dma, dma, dma, dma,
+                dma, dma((4,)), dma, dma,
+                dma, dma((8,)), dma, dma,
+                dma, dma, dma, dma, pltpu.SemaphoreType.REGULAR,
             ],
             compiler_params=pltpu.CompilerParams(
                 collective_id=0, has_side_effects=True, vmem_limit_bytes=56 * 1024 * 1024

time: 44.3 us -> 41.1 us (0.928)
  Pallas kernels: 43.5 us -> 40.3 us
    pallas_call x1, Pallas kernels: 42.5 us -> 39.3 us  [on_device(): pl.pallas_call(functools.partial(kernel, inv_root), out_shape=[pltpu.VMEM...]
where the time goes in v5:
time: 41.1 us; the launch traced here: 40.9 us
  Pallas kernels  40.3 us (98%)
  between operations  0.66 us (2%)
    pallas_call x1, Pallas kernels, on_device(): pl.pallas_call(functools.partial(kernel, inv_root), out_shape=[pltpu.VMEM...  39.3 us
    pallas_call x1, Pallas kernels, on_device(): pl.pallas_call(write_out, out_shape=outs, in_specs=[pl.BlockSpec(memory_s...  0.99 us

profile of v5, /device:TPU:1, one launch (start us, length us, event | category | flops | bytes accessed | tf_op | source)
XLA Modules:
  0.0 40.9 jit_solution(33539321949453681)
XLA Ops:
  0.6 39.3 %shard_map.195 = (f32[16,192]{1,0:T(8,128)S(1)}, f32[32,256]{1,0:T(8,128)S(1)}, f32[16,192]{1,0:T(8,128)S(1)}, f32[32,256]{1,0:T(8,128)S(1)}, bf16[192,512]{1,0:...) custom-call(bf16[3072,512]{1,0:T(8,128)(2,1)} %lat.1, ...), custom_call_target="tpu_custom_call" | custom-call | tf_op jit(solution)/shard_map/pallas_call | solution.py:347
  39.9 1.0 %shard_map.196 = (f32[16,192]{1,0:T(8,128)}, f32[32,256]{1,0:T(8,128)}, f32[16,192]{1,0:T(8,128)}, f32[32,256]{1,0:T(8,128)}, bf16[192,512]{1,0:T(8,128)(2,1)}, ...) custom-call(f32[16,192]{1,0:T(8,128)S(1)} %get-tuple-element.30.refs, ...), custom_call_target="tpu_custom_call" | custom-call | tf_op jit(solution)/shard_map/pallas_call | solution.py:372

commit v6 on v5

--- a/solution.py
+++ b/solution.py
@@ -14,6 +14,8 @@
 NZ, NY = 8, 4
 CHUNKS = 6
 Z_ORDER = (1, 7, 2, 6, 3, 5, 4)
+GROUPS = ((1, 7), (2, 6), (3, 5), (4,))
+GROUP_OF = {k: i for i, ks in enumerate(GROUPS) for k in ks}
 FAR_FIRST = (4, 3, 5, 2, 6, 1, 7)
 BY_DISTANCE = (4, 3, 5, 2, 6, 1, 7, 0)
 PIECES = ((0, 1), (1, 2), (3, 2), (5, 3))
@@ -31,10 +33,9 @@
 def kernel(
     inv_root,
     lat, qcot, att, mix, qw, ow, qf, of, qm, qs, om, os_,
-    sq_v, so_v, nq_v, no_v, cq, co, mq_v, sqq_v, mo_v, soo_v,
-    lat_v, qcot_v, att_v, mix_v, qw_v, ow_v, qm_v, qs_v, om_v, os_v,
-    gq, go, fac, wei, part, part_in, mid, mid_in, drc, sums, sums_in,
-    pq, po,
+    sq_v, so_v, nq_v, no_v, pq, po, wei, scales, mq_v, sqq_v, mo_v, soo_v,
+    rows_v, qcot_v, qw_v, ow_v, mq_in, mo_in,
+    gq, go, gqb, gob, fac, part, part_in, mid, mid_in, drc, sums, sums_in,
     chunk_sem, small_sem,
     fz_s, fz_r, fy_s, fy_r, fd_s, fd_r,
     wz_s, wz_r, wy_s, wy_r, wb_s, wb_r, wc_s, wc_r,
@@ -66,16 +67,19 @@
             src_ref=src, dst_ref=dst, send_sem=send, recv_sem=recv, device_id=to, device_id_type=MESH
         )
 
+    def arrived(ref, sem):
+        pltpu.make_async_copy(ref, ref, sem).wait()
+
+    sent = arrived
     half = pl.ds(pl.multiple_of(core * 128, 128), 128)
     own = fac.at[core, z, y]
-    small = []
-    for i, (src, dst) in enumerate((
-        (qf.at[:, half], own.at[pl.ds(0, 16)]),
-        (of.at[:, half], own.at[pl.ds(16, 32)]),
-        (qw, qw_v), (ow, ow_v), (qm, qm_v), (qs, qs_v), (om, om_v), (os_, os_v),
-    )):
-        small.append(pltpu.make_async_copy(src, dst, small_sem.at[i]))
-        small[-1].start()
+    for src, dst, i in (
+        (qf.at[:, half], own.at[pl.ds(0, 16)], 0),
+        (of.at[:, half], own.at[pl.ds(16, 32)], 0),
+        (qw, qw_v, 1), (ow, ow_v, 2),
+        (qm, mq_in.at[0], 3), (qs, mq_in.at[1], 3), (om, mo_in.at[0], 4), (os_, mo_in.at[1], 4),
+    ):
+        pltpu.make_async_copy(src, dst, small_sem.at[i]).start()
 
     across = [(fs, lax.rem(tp + e, 8)) for e in (4, 2, 6)]
     barrier = pltpu.get_barrier_semaphore()
@@ -84,31 +88,31 @@
 
     tokens = lat.shape[0]
     rows = tokens // CHUNKS
-    pairs = ((lat, lat_v), (mix, mix_v), (att, att_v))
+    pairs = ((lat, pl.ds(0, 512)), (mix, pl.ds(512, 256)), (att, pl.ds(768, 1024)))
 
     def chunk_copies(i):
         span = pl.ds(pl.multiple_of(i * rows, rows), rows)
         copies = [
-            pltpu.make_async_copy(src.at[span], dst.at[span], chunk_sem.at[i, j])
-            for j, (src, dst) in enumerate(pairs)
+            pltpu.make_async_copy(src.at[span], rows_v.at[span, columns], chunk_sem.at[i, 0])
+            for src, columns in pairs
         ]
-        copies.append(pltpu.make_async_copy(qcot.at[:, span], qcot_v.at[:, span], chunk_sem.at[i, 3]))
+        copies.append(pltpu.make_async_copy(qcot.at[:, span], qcot_v.at[:, span], chunk_sem.at[i, 1]))
         return copies
 
     def add_chunk(i):
-        for copy in chunk_copies(i):
-            copy.wait()
         span = pl.ds(pl.multiple_of(i * rows, rows), rows)
-        gq[...] += dot(qcot_v[:, span], lat_v[span, :])
-        go[...] += by_tokens(mix_v[span, :], att_v[span, :])
+        arrived(rows_v.at[span], chunk_sem.at[i, 0])
+        arrived(qcot_v.at[:, span], chunk_sem.at[i, 1])
+        gq[...] += dot(qcot_v[:, span], rows_v[span, 0:512])
+        go[...] += by_tokens(rows_v[span, 512:768], rows_v[span, 768:1792])
 
     def add_chunks(a, b):
         @pl.loop(a, b)
         def _(i):
             add_chunk(i)
 
-    for copy in small[:4]:
-        copy.wait()
+    for i, ref in enumerate((own, qw_v, ow_v)):
+        arrived(ref, small_sem.at[i])
     for i in range(CHUNKS):
         for copy in chunk_copies(i):
             copy.start()
@@ -132,17 +136,9 @@
     def start(copy):
         copy.start()
 
-    def arrived(ref, sem):
-        pltpu.make_async_copy(ref, ref, sem).wait()
-
-    sent = arrived
-
     def z_send(blk, s, r):
         for k in FAR_FIRST:
-            start(remote(blk(z, y), blk(z, y), s, r.at[k], at_z(zup[k])))
-
-    def z_wait(blk, r, k):
-        arrived(blk(zdn[k], y), r.at[k])
+            start(remote(blk(z, y), blk(z, y), s, r.at[GROUP_OF[k]], at_z(zup[k])))
 
     def y_send(blk, s, r, k):
         for d in (2, 1, 3):
@@ -153,7 +149,7 @@
         start(remote(src, src, fd_s, fd_r, partner))
 
     z_send(f_blk, fz_s, fz_r)
-    y_send(f_blk, fy_s, fy_r.at.__getitem__, 0)
+    y_send(f_blk, fy_s, lambda k: fy_r.at[4], 0)
     swap_send(0, 0)
     for d in (2, 1, 3):
         src = wei.at[1, z, y]
@@ -161,20 +157,19 @@
     gq[...] = jnp.zeros_like(gq)
     go[...] = jnp.zeros_like(go)
 
-    def pass_on(k):
-        z_wait(f_blk, fz_r, k)
-        y_send(f_blk, fy_s, fy_r.at.__getitem__, k)
-        swap_send(0, k)
+    def pass_on(g):
+        arrived(fac.at[core, pl.ds(0, len(GROUPS[g])), 0], fz_r.at[g])
+        for k in GROUPS[g]:
+            y_send(f_blk, fy_s, lambda k: fy_r.at[GROUP_OF[k]], k)
+            swap_send(0, k)
 
     add_chunks(0, 3)
-    for k in Z_ORDER[:2]:
-        pass_on(k)
+    pass_on(0)
     add_chunks(3, 4)
-    for k in Z_ORDER[2:4]:
-        pass_on(k)
+    pass_on(1)
     add_chunks(4, 5)
-    for k in Z_ORDER[4:]:
-        pass_on(k)
+    pass_on(2)
+    pass_on(3)
     add_chunks(5, 6)
     for k in FAR_FIRST:
         start(remote(w_blk(z, y), w_blk(z, y), wz_s, wz_r, at_z(zup[k])))
@@ -182,11 +177,13 @@
     for k in FAR_FIRST:
         src = wei.at[1, z]
         start(remote(src, src, wc_s, wc_r, at_z(zup[k])))
-    order = (0,) + Z_ORDER
-    for k in order:
-        arrived(fac.at[core, 0, pl.ds(0, 3)], fy_r.at[k])
-        for d in (1, 3, 2):
-            swap_send(d, k)
+    gqb[...] = gq[...].astype(BF16)
+    gob[...] = go[...].astype(BF16)
+    for g, ks in ((4, (0,)), *enumerate(GROUPS)):
+        arrived(fac.at[core, pl.ds(0, len(ks)), pl.ds(0, 3)], fy_r.at[g])
+        for k in ks:
+            for d in (1, 3, 2):
+                swap_send(d, k)
     arrived(fac.at[other], fd_r)
 
     for to in across:
@@ -196,9 +193,9 @@
             [fac[c, :, :, first:first + count, :].reshape(32 * count, 128) for c in (0, 1)], axis=1
         )
 
-    low_q = dot(gq[...].astype(BF16), factor(0, 16)) * inv_root
+    low_q = dot(gqb[...], factor(0, 16)) * inv_root
     low_q = jnp.concatenate([low_q, jnp.zeros((256 - qcols, 256), F32)], axis=0).T
-    low_o = (dot(go[...].astype(BF16), factor(16, 32)) * inv_root).T
+    low_o = (dot(gob[...], factor(16, 32)) * inv_root).T
     low_q, low_o = low_q.reshape(NZ, NY, 8, 256), low_o.reshape(NZ, NY, 8, 256)
     for lev in range(NZ):
         k = lax.rem(lev + NZ - z, NZ)
@@ -238,10 +235,10 @@
         square_new = 0.9 * square + 0.1 * low * low
         return (mean_new, square_new, mean_new / jnp.sqrt(square_new))
 
-    for copy in small[4:]:
-        copy.wait()
-    mq_v[...], sqq_v[...], dir_q = moments(qm_v[...], qs_v[...], low[0:8, 0:qcols])
-    mo_v[...], soo_v[...], dir_o = moments(om_v[...], os_v[...], low[8:16, :])
+    arrived(mq_in, small_sem.at[3])
+    arrived(mo_in, small_sem.at[4])
+    mq_v[...], sqq_v[...], dir_q = moments(mq_in[0], mq_in[1], low[0:8, 0:qcols])
+    mo_v[...], soo_v[...], dir_o = moments(mo_in[0], mo_in[1], low[8:16, :])
     dir_q = jnp.concatenate([dir_q, jnp.zeros((8, 256 - qcols), F32)], axis=1)
     drc[z, y] = jnp.concatenate([dir_q, dir_o], axis=0).astype(BF16)
     z_send(d_blk, dz_s, dz_r)
@@ -259,12 +256,10 @@
     sent(wei.at[0, pl.ds(0, 7), 0], wz_s)
     sent(part.at[pl.ds(0, 3)], py_s)
     sent(mid.at[pl.ds(0, 7)], pz_s)
-    for k in Z_ORDER[:4]:
-        z_wait(d_blk, dz_r, k)
-        y_send(d_blk, dy_s, lambda k: dy_r, k)
-    for k in Z_ORDER[4:]:
-        z_wait(d_blk, dz_r, k)
-        y_send(d_blk, dy_s, lambda k: dy_r, k)
+    for g, ks in enumerate(GROUPS):
+        arrived(drc.at[pl.ds(0, len(ks)), 0], dz_r.at[g])
+        for k in ks:
+            y_send(d_blk, dy_s, lambda k: dy_r, k)
     arrived(sums_in.at[pl.ds(0, 31)], sx_r)
     total = sums[0] + jnp.sum(sums_in[0:31], axis=0)
     sums[1] = total
@@ -285,42 +280,65 @@
     every = drc[...].astype(F32).reshape(32, 16, 256)
     pq[...] = dot(factor(0, 16), every[:, 0:8].reshape(256, 256).astype(BF16))
     po[...] = dot(factor(16, 32), every[:, 8:16].reshape(256, 256).astype(BF16))
+    arrived(wei.at[0, :, pl.ds(0, 3)], wy_r)
+    arrived(wei.at[1, pl.ds(0, 7)], wc_r)
+    sent(wei.at[1, pl.ds(0, 7)], wc_s)
+    sent(wei.at[0, :, pl.ds(0, 3)], wy_s)
+    sent(drc.at[pl.ds(0, 7), 0], dz_s)
+    sent(drc.at[pl.ds(0, 6)], dy_s)
+    sent(sums_in.at[pl.ds(0, 31)], sx_s)
+
+    @pl.when(core == 1)
+    def _():
+        sent(sums_in.at[pl.ds(0, 14)], sz_s)
+
     arrived(sums_in.at[pl.ds(32, 7)], sz_r)
     total = total + jnp.sum(sums_in[32:39], axis=0)
     count = 256.0 * 8 * qcols
     scale_q = lax.rsqrt(total[0:1, 0:1] / count + 0.25)
     scale_o = lax.rsqrt(total[0:1, 64:65] / (256.0 * 8 * 256) + 0.25)
 
+    scales[...] = jnp.concatenate([jnp.broadcast_to(scale_q, (1, 64)), jnp.broadcast_to(scale_o, (1, 64))], axis=1)
     own_q = pq[pl.ds(pl.multiple_of(fs * 16, 16), 16), :][:, 0:qcols] * scale_q
     own_o = po[pl.ds(pl.multiple_of(fs * 32, 32), 32), :] * scale_o
     sq_v[...] = own_q
     so_v[...] = own_o
     nq_v[...] = qw_v[...] - 0.02 * own_q
     no_v[...] = ow_v[...] - 0.02 * own_o
-    arrived(wei.at[0, :, pl.ds(0, 3)], wy_r)
-    arrived(wei.at[1, pl.ds(0, 7)], wc_r)
-    weights = jnp.concatenate([wei[0].reshape(32, 48, 128), wei[1].reshape(32, 48, 128)], axis=2).astype(F32)
-    weights_q = weights[:, 0:16].reshape(512, 256)
-    weights_o = weights[:, 16:48].reshape(1024, 256)
-    cq[...] = (weights_q - 0.02 * (pq[...] * scale_q)).T[0:qcols, :].astype(BF16)
-    co[...] = (weights_o - 0.02 * (po[...] * scale_o)).astype(BF16)
-    sent(wei.at[1, pl.ds(0, 7)], wc_s)
-    sent(wei.at[0, :, pl.ds(0, 3)], wy_s)
-    sent(drc.at[pl.ds(0, 7), 0], dz_s)
-    sent(drc.at[pl.ds(0, 6)], dy_s)
-    sent(sums_in.at[pl.ds(0, 31)], sx_s)
-
-    @pl.when(core == 1)
-    def _():
-        sent(sums_in.at[pl.ds(0, 14)], sz_s)
-
-
-def write_out(*refs):
-    n = len(refs) // 2
-    sem = refs[-1]
-    copies = [pltpu.make_async_copy(refs[i], refs[n + i], sem.at[i]) for i in range(n)]
-    for copy in copies:
-        copy.start()
+
+
+def write_out(
+    sq_v, so_v, nq_v, no_v, pq, po, wei, scales, mq_v, sqq_v, mo_v, soo_v,
+    step_q, step_o, new_q, new_o, copy_q, copy_o, mean_q, square_q, mean_o, square_o,
+    cq, co, sem,
+):
+    copies = []
+
+    def put(src, dst):
+        copies.append(pltpu.make_async_copy(src, dst, sem.at[len(copies)]))
+        copies[-1].start()
+
+    for src, dst in (
+        (sq_v, step_q), (so_v, step_o), (nq_v, new_q), (no_v, new_o),
+        (mq_v, mean_q), (sqq_v, square_q), (mo_v, mean_o), (soo_v, square_o),
+    ):
+        put(src, dst)
+    scale_q, scale_o = scales[0:1, 0:1], scales[0:1, 64:65]
+
+    def weights(levels, rows):
+        halves = [wei[i, levels, :, rows, :] for i in (0, 1)]
+        both = jnp.concatenate([h.reshape(-1, 128) for h in halves], axis=1)
+        return both.astype(F32)
+
+    for j in range(4):
+        span = pl.ds(256 * j, 256)
+        old = weights(slice(2 * j, 2 * j + 2), slice(16, 48))
+        co[span, :] = (old - 0.02 * (po[span, :] * scale_o)).astype(BF16)
+        put(co.at[span], copy_o.at[span])
+        if j == 1:
+            old = weights(slice(0, NZ), slice(0, 16))
+            cq[...] = (old - 0.02 * (pq[...] * scale_q)).T[0:cq.shape[0], :].astype(BF16)
+            put(cq, copy_q)
     for copy in copies:
         copy.wait()
 
@@ -343,26 +361,31 @@
             jax.ShapeDtypeStruct((qcols, 512), BF16), jax.ShapeDtypeStruct((1024, 256), BF16),
             like(qm), like(qs), like(om), like(os_),
         )
+        kept = [vm(qw), vm(ow), vm(qw), vm(ow)]
+        kept += [pltpu.VMEM((512, 256), F32), pltpu.VMEM((1024, 256), F32)]
+        kept += [pltpu.VMEM((2, NZ, NY, 48, 128), BF16), pltpu.VMEM((1, 128), F32)]
+        kept += [vm(qm), vm(qs), vm(om), vm(os_)]
         qcot = qcot.T
         held = pl.pallas_call(
             functools.partial(kernel, inv_root),
-            out_shape=[pltpu.VMEM(a.shape, a.dtype) for a in outs],
+            out_shape=kept,
             in_specs=[any_] * 12,
-            out_specs=[pl.BlockSpec(memory_space=pltpu.VMEM)] * 10,
+            out_specs=[pl.BlockSpec(memory_space=pltpu.VMEM)] * 12,
             scratch_shapes=[
-                vm(lat), vm(qcot), vm(att), vm(mix), vm(qw), vm(ow), vm(qm), vm(qs), vm(om), vm(os_),
+                pltpu.VMEM((tokens, 1792), BF16), vm(qcot), vm(qw), vm(ow),
+                pltpu.VMEM((2, 8, qcols), F32), pltpu.VMEM((2, 8, 256), F32),
                 pltpu.VMEM((qcols, 512), F32), pltpu.VMEM((256, 1024), F32),
-                pltpu.VMEM((2, NZ, NY, 48, 128), BF16), pltpu.VMEM((2, NZ, NY, 48, 128), BF16),
+                pltpu.VMEM((qcols, 512), BF16), pltpu.VMEM((256, 1024), BF16),
+                pltpu.VMEM((2, NZ, NY, 48, 128), BF16),
                 pltpu.VMEM((NY, NZ, 16, 256), BF16), pltpu.VMEM((NY, NZ, 16, 256), BF16),
                 pltpu.VMEM((NZ, 16, 256), BF16), pltpu.VMEM((NZ, 16, 256), BF16),
                 pltpu.VMEM((NZ, NY, 16, 256), BF16),
                 pltpu.VMEM((2, 1, 128), F32), pltpu.VMEM((39, 1, 128), F32),
-                pltpu.VMEM((512, 256), F32), pltpu.VMEM((1024, 256), F32),
-                dma((CHUNKS, 4)), dma((8,)),
-                dma, dma((8,)), dma, dma((8,)), dma, dma,
+                dma((CHUNKS, 2)), dma((5,)),
+                dma, dma((4,)), dma, dma((5,)), dma, dma,
                 dma, dma, dma, dma, dma, dma, dma, dma,
                 dma, dma((4,)), dma, dma,
-                dma, dma((8,)), dma, dma,
+                dma, dma((4,)), dma, dma,
                 dma, dma, dma, dma, pltpu.SemaphoreType.REGULAR,
             ],
             compiler_params=pltpu.CompilerParams(
@@ -372,9 +395,9 @@
         results = pl.pallas_call(
             write_out,
             out_shape=outs,
-            in_specs=[pl.BlockSpec(memory_space=pltpu.VMEM)] * 10,
+            in_specs=[pl.BlockSpec(memory_space=pltpu.VMEM)] * 12,
             out_specs=[any_] * 10,
-            scratch_shapes=[dma((10,))],
+            scratch_shapes=[pltpu.VMEM((qcols, 512), BF16), pltpu.VMEM((1024, 256), BF16), dma((13,))],
         )(*[pltpu.with_memory_space_constraint(a, pltpu.VMEM) for a in held])
         return (*results[:4], results[4].T, *results[5:])
 

time: 41.1 us -> 40.6 us (0.988)
  Pallas kernels: 40.3 us -> 39.8 us
    pallas_call x1, Pallas kernels: 39.3 us -> 38.6 us  [on_device(): pl.pallas_call(functools.partial(kernel, inv_root), out_shape=kept, in_sp...]
where the time goes in v6:
time: 40.6 us; the launch traced here: 40.5 us
  Pallas kernels  39.8 us (98%)
  between operations  0.66 us (2%)
    pallas_call x1, Pallas kernels, on_device(): pl.pallas_call(functools.partial(kernel, inv_root), out_shape=kept, in_sp...  38.6 us
    pallas_call x1, Pallas kernels, on_device(): pl.pallas_call(write_out, out_shape=outs, in_specs=[pl.BlockSpec(memory_s...  1.26 us

profile of v6, /device:TPU:1, one launch (start us, length us, event | category | flops | bytes accessed | tf_op | source)
XLA Modules:
  0.0 40.5 jit_solution(14713878012118896764)
XLA Ops:
  0.6 38.6 %shard_map.195 = (f32[16,192]{1,0:T(8,128)S(1)}, f32[32,256]{1,0:T(8,128)S(1)}, f32[16,192]{1,0:T(8,128)S(1)}, f32[32,256]{1,0:T(8,128)S(1)}, f32[512,256]{1,0:T...) custom-call(bf16[3072,512]{1,0:T(8,128)(2,1)} %lat.1, ...), custom_call_target="tpu_custom_call" | custom-call | tf_op jit(solution)/shard_map/pallas_call | solution.py:369
  39.2 1.3 %shard_map.196 = (f32[16,192]{1,0:T(8,128)}, f32[32,256]{1,0:T(8,128)}, f32[16,192]{1,0:T(8,128)}, f32[32,256]{1,0:T(8,128)}, bf16[192,512]{1,0:T(8,128)(2,1)}, ...) custom-call(f32[16,192]{1,0:T(8,128)S(1)} %get-tuple-element.32.sq_v, ...), custom_call_target="tpu_custom_call" | custom-call | tf_op jit(solution)/shard_map/pallas_call | solution.py:395

commit v7 on v6

--- a/solution.py
+++ b/solution.py
@@ -117,18 +117,18 @@
         for copy in chunk_copies(i):
             copy.start()
     qcols = qw_v.shape[1]
-    wei[0, z, y, 0:16] = qw_v[:, 0:128].astype(BF16)
-    wei[1, z, y, 0:16, 0:qcols - 128] = qw_v[:, 128:qcols].astype(BF16)
-    for i in (0, 1):
-        wei[i, z, y, 16:48] = ow_v[:, 128 * i:128 * i + 128].astype(BF16)
+    wei[z, y, 0:16, 0:qcols] = qw_v[...].astype(BF16)
+    wei[z, y, 16:48] = ow_v[...].astype(BF16)
 
     pl.semaphore_wait(barrier, 14)
 
     def f_blk(level, row):
         return fac.at[core, level, row]
 
+    q_rows, o_rows = pl.ds(0, 16), pl.ds(16, 32)
+
     def w_blk(level, row):
-        return wei.at[0, level, row]
+        return wei.at[level, row, o_rows]
 
     def d_blk(level, row):
         return drc.at[level, row]
@@ -152,7 +152,7 @@
     y_send(f_blk, fy_s, lambda k: fy_r.at[4], 0)
     swap_send(0, 0)
     for d in (2, 1, 3):
-        src = wei.at[1, z, y]
+        src = wei.at[z, y, q_rows]
         start(remote(src, src, wb_s, wb_r, at_y(ups[d])))
     gq[...] = jnp.zeros_like(gq)
     go[...] = jnp.zeros_like(go)
@@ -173,9 +173,9 @@
     add_chunks(5, 6)
     for k in FAR_FIRST:
         start(remote(w_blk(z, y), w_blk(z, y), wz_s, wz_r, at_z(zup[k])))
-    arrived(wei.at[1, 0, pl.ds(0, 3)], wb_r)
+    arrived(wei.at[0, pl.ds(0, 3), q_rows], wb_r)
     for k in FAR_FIRST:
-        src = wei.at[1, z]
+        src = wei.at[z, :, q_rows]
         start(remote(src, src, wc_s, wc_r, at_z(zup[k])))
     gqb[...] = gq[...].astype(BF16)
     gob[...] = go[...].astype(BF16)
@@ -221,9 +221,9 @@
             if k:
                 start(remote(mid.at[j], mid_in.at[k], pz_s, pz_r, at_z(zup[k])))
     pl.semaphore_wait(met, 3)
-    arrived(wei.at[0, pl.ds(0, 7), 0], wz_r)
+    arrived(wei.at[pl.ds(0, 7), 0, o_rows], wz_r)
     for d in (2, 1, 3):
-        src = wei.at[0, :, y]
+        src = wei.at[:, y, o_rows]
         start(remote(src, src, wy_s, wy_r, at_y(ups[d])))
     arrived(mid_in.at[pl.ds(1, 7)], pz_r)
     low = mid[7].astype(F32)
@@ -241,19 +241,19 @@
     mo_v[...], soo_v[...], dir_o = moments(mo_in[0], mo_in[1], low[8:16, :])
     dir_q = jnp.concatenate([dir_q, jnp.zeros((8, 256 - qcols), F32)], axis=1)
     drc[z, y] = jnp.concatenate([dir_q, dir_o], axis=0).astype(BF16)
-    z_send(d_blk, dz_s, dz_r)
-    y_send(d_blk, dy_s, lambda k: dy_r, 0)
-
     sum_q = jnp.sum(dir_q * dir_q, axis=(0, 1), keepdims=True)
     sum_o = jnp.sum(dir_o * dir_o, axis=(0, 1), keepdims=True)
     sums[0] = jnp.concatenate([jnp.broadcast_to(sum_q, (1, 64)), jnp.broadcast_to(sum_o, (1, 64))], axis=1)
     for i, (d, e) in enumerate(SIDE):
         start(remote(sums.at[0], sums_in.at[i], sx_s, sx_r, side(d, e)))
+    z_send(d_blk, dz_s, dz_r)
+    y_send(d_blk, dy_s, lambda k: dy_r, 0)
+
     sent(fac.at[core, pl.ds(0, 7), 0], fz_s)
     sent(fac.at[core, pl.ds(0, 6)], fy_s)
     sent(fac.at[core], fd_s)
-    sent(wei.at[1, 0, pl.ds(0, 3)], wb_s)
-    sent(wei.at[0, pl.ds(0, 7), 0], wz_s)
+    sent(wei.at[0, pl.ds(0, 3), q_rows], wb_s)
+    sent(wei.at[pl.ds(0, 7), 0, o_rows], wz_s)
     sent(part.at[pl.ds(0, 3)], py_s)
     sent(mid.at[pl.ds(0, 7)], pz_s)
     for g, ks in enumerate(GROUPS):
@@ -280,10 +280,10 @@
     every = drc[...].astype(F32).reshape(32, 16, 256)
     pq[...] = dot(factor(0, 16), every[:, 0:8].reshape(256, 256).astype(BF16))
     po[...] = dot(factor(16, 32), every[:, 8:16].reshape(256, 256).astype(BF16))
-    arrived(wei.at[0, :, pl.ds(0, 3)], wy_r)
-    arrived(wei.at[1, pl.ds(0, 7)], wc_r)
-    sent(wei.at[1, pl.ds(0, 7)], wc_s)
-    sent(wei.at[0, :, pl.ds(0, 3)], wy_s)
+    arrived(wei.at[:, pl.ds(0, 3), o_rows], wy_r)
+    arrived(wei.at[pl.ds(0, 7), :, q_rows], wc_r)
+    sent(wei.at[pl.ds(0, 7), :, q_rows], wc_s)
+    sent(wei.at[:, pl.ds(0, 3), o_rows], wy_s)
     sent(drc.at[pl.ds(0, 7), 0], dz_s)
     sent(drc.at[pl.ds(0, 6)], dy_s)
     sent(sums_in.at[pl.ds(0, 31)], sx_s)
@@ -326,9 +326,7 @@
     scale_q, scale_o = scales[0:1, 0:1], scales[0:1, 64:65]
 
     def weights(levels, rows):
-        halves = [wei[i, levels, :, rows, :] for i in (0, 1)]
-        both = jnp.concatenate([h.reshape(-1, 128) for h in halves], axis=1)
-        return both.astype(F32)
+        return wei[levels, :, rows, :].reshape(-1, 256).astype(F32)
 
     for j in range(4):
         span = pl.ds(256 * j, 256)
@@ -363,7 +361,7 @@
         )
         kept = [vm(qw), vm(ow), vm(qw), vm(ow)]
         kept += [pltpu.VMEM((512, 256), F32), pltpu.VMEM((1024, 256), F32)]
-        kept += [pltpu.VMEM((2, NZ, NY, 48, 128), BF16), pltpu.VMEM((1, 128), F32)]
+        kept += [pltpu.VMEM((NZ, NY, 48, 256), BF16), pltpu.VMEM((1, 128), F32)]
         kept += [vm(qm), vm(qs), vm(om), vm(os_)]
         qcot = qcot.T
         held = pl.pallas_call(

time: 40.6 us -> 40.2 us (level)
    pallas_call x1, Pallas kernels: 38.6 us -> 38.1 us  [on_device(): pl.pallas_call(functools.partial(kernel, inv_root), out_shape=kept, in_sp...]
where the time goes in v7:
time: 40.2 us; the launch traced here: 40 us
  Pallas kernels  39.4 us (98%)
  between operations  0.66 us (2%)
    pallas_call x1, Pallas kernels, on_device(): pl.pallas_call(functools.partial(kernel, inv_root), out_shape=kept, in_sp...  38.1 us
    pallas_call x1, Pallas kernels, on_device(): pl.pallas_call(write_out, out_shape=outs, in_specs=[pl.BlockSpec(memory_s...  1.26 us

profile of v7, /device:TPU:1, one launch (start us, length us, event | category | flops | bytes accessed | tf_op | source)
XLA Modules:
  0.0 40.0 jit_solution(2774235804205211586)
XLA Ops:
  0.6 38.1 %shard_map.195 = (f32[16,192]{1,0:T(8,128)S(1)}, f32[32,256]{1,0:T(8,128)S(1)}, f32[16,192]{1,0:T(8,128)S(1)}, f32[32,256]{1,0:T(8,128)S(1)}, f32[512,256]{1,0:T...) custom-call(bf16[3072,512]{1,0:T(8,128)(2,1)} %lat.1, ...), custom_call_target="tpu_custom_call" | custom-call | tf_op jit(solution)/shard_map/pallas_call | solution.py:367
  38.8 1.3 %shard_map.196 = (f32[16,192]{1,0:T(8,128)}, f32[32,256]{1,0:T(8,128)}, f32[16,192]{1,0:T(8,128)}, f32[32,256]{1,0:T(8,128)}, bf16[192,512]{1,0:T(8,128)(2,1)}, ...) custom-call(f32[16,192]{1,0:T(8,128)S(1)} %get-tuple-element.32.sq_v, ...), custom_call_target="tpu_custom_call" | custom-call | tf_op jit(solution)/shard_map/pallas_call | solution.py:393

commit v8 on v7

--- a/solution.py
+++ b/solution.py
@@ -220,11 +220,12 @@
             k = BY_DISTANCE[j]
             if k:
                 start(remote(mid.at[j], mid_in.at[k], pz_s, pz_r, at_z(zup[k])))
+        if i == 2:
+            arrived(wei.at[pl.ds(0, 7), 0, o_rows], wz_r)
+            for d in (2, 1, 3):
+                src = wei.at[:, y, o_rows]
+                start(remote(src, src, wy_s, wy_r, at_y(ups[d])))
     pl.semaphore_wait(met, 3)
-    arrived(wei.at[pl.ds(0, 7), 0, o_rows], wz_r)
-    for d in (2, 1, 3):
-        src = wei.at[:, y, o_rows]
-        start(remote(src, src, wy_s, wy_r, at_y(ups[d])))
     arrived(mid_in.at[pl.ds(1, 7)], pz_r)
     low = mid[7].astype(F32)
     for k in Z_ORDER:

time: 40.2 us -> 39.5 us (0.983)
  Pallas kernels: 39.4 us -> 38.7 us
    pallas_call x1, Pallas kernels: 38.1 us -> 37.4 us  [on_device(): pl.pallas_call(functools.partial(kernel, inv_root), out_shape=kept, in_sp...]
where the time goes in v8:
time: 39.5 us; the launch traced here: 39.3 us
  Pallas kernels  38.7 us (98%)
  between operations  0.66 us (2%)
    pallas_call x1, Pallas kernels, on_device(): pl.pallas_call(functools.partial(kernel, inv_root), out_shape=kept, in_sp...  37.4 us
    pallas_call x1, Pallas kernels, on_device(): pl.pallas_call(write_out, out_shape=outs, in_specs=[pl.BlockSpec(memory_s...  1.26 us

profile of v8, /device:TPU:1, one launch (start us, length us, event | category | flops | bytes accessed | tf_op | source)
XLA Modules:
  0.0 39.3 jit_solution(3633164100126931021)
XLA Ops:
  0.6 37.4 %shard_map.195 = (f32[16,192]{1,0:T(8,128)S(1)}, f32[32,256]{1,0:T(8,128)S(1)}, f32[16,192]{1,0:T(8,128)S(1)}, f32[32,256]{1,0:T(8,128)S(1)}, f32[512,256]{1,0:T...) custom-call(bf16[3072,512]{1,0:T(8,128)(2,1)} %lat.1, ...), custom_call_target="tpu_custom_call" | custom-call | tf_op jit(solution)/shard_map/pallas_call | solution.py:368
  38.1 1.3 %shard_map.196 = (f32[16,192]{1,0:T(8,128)}, f32[32,256]{1,0:T(8,128)}, f32[16,192]{1,0:T(8,128)}, f32[32,256]{1,0:T(8,128)}, bf16[192,512]{1,0:T(8,128)(2,1)}, ...) custom-call(f32[16,192]{1,0:T(8,128)S(1)} %get-tuple-element.32.sq_v, ...), custom_call_target="tpu_custom_call" | custom-call | tf_op jit(solution)/shard_map/pallas_call | solution.py:394

commit v9 on v8

--- a/solution.py
+++ b/solution.py
@@ -163,13 +163,9 @@
             y_send(f_blk, fy_s, lambda k: fy_r.at[GROUP_OF[k]], k)
             swap_send(0, k)
 
-    add_chunks(0, 3)
-    pass_on(0)
-    add_chunks(3, 4)
-    pass_on(1)
-    add_chunks(4, 5)
-    pass_on(2)
-    pass_on(3)
+    add_chunks(0, 5)
+    for g in range(len(GROUPS)):
+        pass_on(g)
     add_chunks(5, 6)
     for k in FAR_FIRST:
         start(remote(w_blk(z, y), w_blk(z, y), wz_s, wz_r, at_z(zup[k])))

time: 39.5 us -> 39.6 us (level)
  no operation moved by 1% of the time
where the time goes in v9:
time: 39.6 us; the launch traced here: 39.4 us
  Pallas kernels  38.8 us (98%)
  between operations  0.66 us (2%)
    pallas_call x1, Pallas kernels, on_device(): pl.pallas_call(functools.partial(kernel, inv_root), out_shape=kept, in_sp...  37.5 us
    pallas_call x1, Pallas kernels, on_device(): pl.pallas_call(write_out, out_shape=outs, in_specs=[pl.BlockSpec(memory_s...  1.26 us

profile of v9, /device:TPU:1, one launch (start us, length us, event | category | flops | bytes accessed | tf_op | source)
XLA Modules:
  0.0 39.4 jit_solution(14770326799148737433)
XLA Ops:
  0.6 37.5 %shard_map.195 = (f32[16,192]{1,0:T(8,128)S(1)}, f32[32,256]{1,0:T(8,128)S(1)}, f32[16,192]{1,0:T(8,128)S(1)}, f32[32,256]{1,0:T(8,128)S(1)}, f32[512,256]{1,0:T...) custom-call(bf16[3072,512]{1,0:T(8,128)(2,1)} %lat.1, ...), custom_call_target="tpu_custom_call" | custom-call | tf_op jit(solution)/shard_map/pallas_call | solution.py:364
  38.2 1.3 %shard_map.196 = (f32[16,192]{1,0:T(8,128)}, f32[32,256]{1,0:T(8,128)}, f32[16,192]{1,0:T(8,128)}, f32[32,256]{1,0:T(8,128)}, bf16[192,512]{1,0:T(8,128)(2,1)}, ...) custom-call(f32[16,192]{1,0:T(8,128)S(1)} %get-tuple-element.32.sq_v, ...), custom_call_target="tpu_custom_call" | custom-call | tf_op jit(solution)/shard_map/pallas_call | solution.py:390
